TPU v7x, 32 devices: a whole 2x2x4 slice. The times are simulated.
32 devices in a mesh: ep: 8 (over z, x), tp: 4 (over y, core).
Axes of the slice: x: 2, y: 2, z: 4, core: 2. Of those that a mesh axis runs over, the one named last changes fastest.
Arguments:
- mixer_input: bfloat16 [2048, 2048], P('ep'), may hold values from -6 to 6
- mixer_gain: float32 [2048], replicated, may hold values from 0.1 to 8
- query_one: bfloat16 [2048, 512], P(None, 'tp'), may hold values from -0.1875 to 0.1875
- query_two: bfloat16 [2048, 512], P(None, 'tp'), may hold values from -0.1875 to 0.1875
- key_one: bfloat16 [2048, 256], P(None, 'tp'), may hold values from -0.1875 to 0.1875
- key_two: bfloat16 [2048, 256], P(None, 'tp'), may hold values from -0.1875 to 0.1875
- value_weight: bfloat16 [2048, 512], P(None, 'tp'), may hold values from -0.125 to 0.125
- lambdas: float32 [8], P('tp'), may hold values from 0.3 to 0.8
- head_gain: float32 [128], replicated, may hold values from 0.1 to 1.9
- output_weight: bfloat16 [1024, 2048], P('tp'), may hold values from -0.1875 to 0.1875
- expert_input: bfloat16 [4096, 2048], P(('ep', 'tp')), may hold values from -6 to 6
- expert_gain: float32 [2048], replicated, may hold values from 0.1 to 1.9
- routes: int32 [4096, 2], P(('ep', 'tp')), may hold values from 0 to 7, all different within a row; in each aligned block of 128 rows (0 to 127, 128 to 255, ...) at most 40 rows name the same one
- route_weight: float32 [4096, 2], P(('ep', 'tp')), may hold values from 0.2 to 1
- expert_gate: bfloat16 [8, 2048, 1024], P('ep', None, 'tp'), may hold values from -0.125 to 0.125
- expert_up: bfloat16 [8, 2048, 1024], P('ep', None, 'tp'), may hold values from -0.125 to 0.125
- expert_down: bfloat16 [8, 1024, 2048], P('ep', 'tp'), may hold values from -0.1875 to 0.1875
- shared_gate: bfloat16 [2048, 512], P(None, 'tp'), may hold values from -0.125 to 0.125
- shared_up: bfloat16 [2048, 512], P(None, 'tp'), may hold values from -0.125 to 0.125
- shared_down: bfloat16 [512, 2048], P('tp'), may hold values from -0.25 to 0.25
Outputs:
- mixer_output: bfloat16 [2048, 2048], P(('ep', 'tp'))
- expert_output: bfloat16 [4096, 2048], P(('ep', 'tp'))
Inputs may be any that keep to these rules, and one draw needn't show every extreme that they name: `routes`: each row names 2 different experts; in the rows of one device no expert is named by more than 40 rows, and some device names some expert exactly 40 times.
All inputs are finite; a program needn't handle non-finite values.
Results may differ from a plain program's by a relative error of at most 0.014.
The roundings to bfloat16 on the way count: a program that leaves them out, or rounds other values in their place, can miss the bound.
Values may be sent and summed in bfloat16 or wider, within the bound.
No kernel may reach another device: no remote copies, remote signals or barrier semaphores. Data moves between devices by JAX's collectives and lax.ppermute only.
A program may use at most 128 MiB of HBM per device.

v0:
```python
import jax
import jax.numpy as jnp
from jax import lax
from jax.experimental import pallas as pl
from jax.experimental.pallas import tpu as pltpu
from jax.sharding import PartitionSpec as P


HEAD = 64
EPS = 1e-06
NEG = -1e30
MOST_PERMUTES = 8


def normalize(activations, scaling):
    values = activations.astype(jnp.float32)
    factor = lax.rsqrt(jnp.mean(values * values, axis=-1, keepdims=True) + EPS)
    return (values * factor * scaling).astype(jnp.bfloat16)


def rotate(chunk, axis, size, shift):
    return lax.ppermute(chunk, axis, [(i, (i + shift) % size) for i in range(size)])


def exchange(chunks, rank, size, sign):
    if size <= MOST_PERMUTES:
        return [chunks[0]] + [
            rotate(chunk, "ep", size, sign * k) for k, chunk in enumerate(chunks) if k
        ]
    order = (sign * (jnp.arange(size, dtype=jnp.int32) - rank)) % size
    arrived = lax.all_to_all(
        jnp.stack(chunks)[order], "ep", split_axis=0, concat_axis=0, tiled=True
    )
    back = (rank - sign * jnp.arange(size, dtype=jnp.int32)) % size
    arrived = arrived[back]
    return [arrived.reshape(-1, arrived.shape[-1])]


VMEM = pl.BlockSpec(memory_space=pltpu.VMEM)
SMEM = pl.BlockSpec(memory_space=pltpu.SMEM)


def project_kernel(rows_ref, gain_ref, one, two, key_one, key_two, value, query_ref, kv_ref):
    values = rows_ref[...].astype(jnp.float32)
    factor = lax.rsqrt(jnp.mean(values * values, axis=-1, keepdims=True) + EPS)
    normed = (values * factor * gain_ref[...]).astype(jnp.bfloat16)

    def plain(weight):
        return jnp.dot(normed, weight[...], preferred_element_type=jnp.float32).astype(jnp.bfloat16)

    def turned(weight):
        return lax.dot_general(
            normed, weight[...], (((1,), (1,)), ((), ())), preferred_element_type=jnp.float32
        ).astype(jnp.bfloat16)

    query_ref[...] = jnp.concatenate([plain(one), plain(two)], axis=1)
    kv_ref[...] = jnp.concatenate([turned(key_one), turned(key_two), plain(value)], axis=1)


def project(rows, gain, one, two, key_one, key_two, value):
    count = rows.shape[0]
    kv_cols = 2 * key_one.shape[1] + value.shape[1]
    return pl.pallas_call(
        project_kernel,
        out_shape=(
            jax.ShapeDtypeStruct((count, 2 * one.shape[1]), jnp.bfloat16),
            jax.ShapeDtypeStruct((count, kv_cols), jnp.bfloat16),
        ),
        in_specs=[VMEM] * 7,
        out_specs=(VMEM, VMEM),
        cost_estimate=pl.CostEstimate(
            flops=2_000_000_000, transcendentals=1000, bytes_accessed=4_000_000
        ),
        name="project",
    )(rows, gain.reshape(1, -1), one, two, key_one.T, key_two.T, value)


def stack(chunks):
    if len(chunks) == 1:
        return chunks[0]
    rows, width = chunks[0].shape

    def kernel(*refs):
        for k, ref in enumerate(refs[:-1]):
            refs[-1][k] = ref[...]

    return pl.pallas_call(
        kernel,
        out_shape=jax.ShapeDtypeStruct((len(chunks), rows, width), chunks[0].dtype),
        in_specs=[VMEM] * len(chunks),
        out_specs=VMEM,
        name="stack",
    )(*chunks).reshape(-1, width)


def routed_part(rows, gates, ups, downs, earlier, last):
    count = len(gates)

    def kernel(*refs):
        rows_ref, out_ref = refs[0], refs[-1]
        gate_refs = refs[1 : 1 + count]
        up_refs = refs[1 + count : 1 + 2 * count]
        down_refs = refs[1 + 2 * count : 1 + 3 * count]
        inputs = rows_ref[...]
        hidden = []
        for gate, up in zip(gate_refs, up_refs):
            gated = jnp.dot(inputs, gate[...], preferred_element_type=jnp.float32)
            lifted = jnp.dot(inputs, up[...], preferred_element_type=jnp.float32)
            hidden.append((jax.nn.silu(gated) * lifted).astype(jnp.bfloat16))
        total = None if earlier is None else refs[1 + 3 * count][...]
        for units, down in zip(hidden, down_refs):
            part = jnp.dot(units, down[...], preferred_element_type=jnp.float32)
            part = part.astype(jnp.bfloat16).astype(jnp.float32)
            total = part if total is None else total + part
        out_ref[...] = total.astype(out_ref.dtype)

    operands = [rows, *gates, *ups, *downs] + ([] if earlier is None else [earlier])
    return pl.pallas_call(
        kernel,
        out_shape=jax.ShapeDtypeStruct(rows.shape, jnp.bfloat16 if last else jnp.float32),
        in_specs=[VMEM] * len(operands),
        out_specs=VMEM,
        cost_estimate=pl.CostEstimate(
            flops=count * 2_000_000_000, transcendentals=1000, bytes_accessed=8_000_000
        ),
        compiler_params=pltpu.CompilerParams(vmem_limit_bytes=48 * 1024 * 1024),
        name="routed",
    )(*operands)


def tp_blocks(shard, size):
    blocks = [shard]
    bit = size // 2
    while bit:
        pairs = [(i, i ^ bit) for i in range(size)]
        blocks = blocks + [lax.ppermute(block, "tp", pairs) for block in blocks]
        bit //= 2
    return blocks


def attention_kernel(
    rank_ref,
    lambda_ref,
    query_ref,
    own_ref,
    gain_ref,
    weight_ref,
    *rest,
    local_kv,
    group,
    value_dim,
):
    out_ref, maxima, totals, weighted = rest[-4:]
    others = rest[:-4]
    rows = query_ref.shape[0]
    key_cols = local_kv * HEAD
    query_cols = key_cols * group

    def stacked(head, which):
        first = which * query_cols + head * group * HEAD
        return jnp.concatenate(
            [query_ref[:, first + g * HEAD : first + (g + 1) * HEAD] for g in range(group)], axis=0
        ) * jnp.bfloat16(HEAD ** (-0.5))

    queries = [[stacked(head, which) for which in range(2)] for head in range(local_kv)]

    def block(keys, head, which):
        key_part = keys[:, which * key_cols + head * HEAD : which * key_cols + (head + 1) * HEAD]
        value_part = keys[
            :, 2 * key_cols + head * value_dim : 2 * key_cols + (head + 1) * value_dim
        ]
        scores = lax.dot_general(
            queries[head][which],
            key_part,
            (((1,), (1,)), ((), ())),
            preferred_element_type=jnp.float32,
        )
        return scores, value_part

    own = own_ref[...]
    position = lax.broadcasted_iota(jnp.int32, (group * rows, rows), 0) % rows
    visible = lax.broadcasted_iota(jnp.int32, (group * rows, rows), 1) <= position
    for head in range(local_kv):
        for which in range(2):
            slot = head * 2 + which
            scores, value_part = block(own, head, which)
            scores = jnp.where(visible, scores, NEG)
            highest = jnp.max(scores, axis=-1, keepdims=True)
            weights = jnp.exp(scores - highest)
            maxima[slot] = highest
            totals[slot] = jnp.sum(weights, axis=-1, keepdims=True)
            weighted[slot] = jnp.dot(
                weights.astype(jnp.bfloat16), value_part, preferred_element_type=jnp.float32
            )

    def earlier_block(keys):
        for head in range(local_kv):
            for which in range(2):
                slot = head * 2 + which
                scores, value_part = block(keys, head, which)
                before = maxima[slot]
                highest = jnp.maximum(before, jnp.max(scores, axis=-1, keepdims=True))
                shrink = jnp.exp(before - highest)
                weights = jnp.exp(scores - highest)
                maxima[slot] = highest
                totals[slot] = totals[slot] * shrink + jnp.sum(weights, axis=-1, keepdims=True)
                weighted[slot] = weighted[slot] * shrink + jnp.dot(
                    weights.astype(jnp.bfloat16), value_part, preferred_element_type=jnp.float32
                )

    if len(others) > 1:
        for step, other in enumerate(others):
            pl.when(step < rank_ref[0])(lambda other=other: earlier_block(other[...]))
    else:

        def one_step(step, carry):
            earlier_block(others[0][step])
            return carry

        lax.fori_loop(0, rank_ref[0], one_step, 0)
    parts = []
    for head in range(local_kv):
        first = weighted[head * 2] / totals[head * 2]
        second = weighted[head * 2 + 1] / totals[head * 2 + 1]
        for g in range(group):
            span = slice(g * rows, (g + 1) * rows)
            combined = first[span] - lambda_ref[head * group + g] * second[span]
            factor = lax.rsqrt(jnp.mean(combined * combined, axis=-1, keepdims=True) + EPS)
            parts.append((combined * factor * gain_ref[...]).astype(jnp.bfloat16))
    head_rows = jnp.concatenate(parts, axis=1)
    out_ref[...] = jnp.dot(
        head_rows, weight_ref[...], preferred_element_type=jnp.float32
    ).astype(jnp.bfloat16)


def attention(rank, lambdas, queries, own, others, head_gain, output_weight, local_kv, group):
    rows = queries.shape[0]
    value_dim = head_gain.shape[0]
    kernel = lambda *refs: attention_kernel(
        *refs, local_kv=local_kv, group=group, value_dim=value_dim
    )
    stats = (2 * local_kv, group * rows, 1)
    return pl.pallas_call(
        kernel,
        out_shape=jax.ShapeDtypeStruct((rows, output_weight.shape[1]), jnp.bfloat16),
        in_specs=[SMEM, SMEM] + [VMEM] * (4 + len(others)),
        out_specs=VMEM,
        scratch_shapes=[
            pltpu.VMEM(stats, jnp.float32),
            pltpu.VMEM(stats, jnp.float32),
            pltpu.VMEM((2 * local_kv, group * rows, value_dim), jnp.float32),
        ],
        cost_estimate=pl.CostEstimate(
            flops=6_000_000_000, transcendentals=4_000_000, bytes_accessed=4_000_000
        ),
        name="attention",
    )(rank.reshape(1), lambdas, queries, own, head_gain.reshape(1, -1), output_weight, *others)


def combine_kernel(slot_ref, weight_ref, shared_ref, *rest):
    out_ref = rest[-1]
    returned = rest[0][...] if len(rest) == 2 else jnp.concatenate([r[...] for r in rest[:-1]], 0)
    tokens, top = slot_ref.shape
    places = lax.broadcasted_iota(jnp.int32, (tokens, returned.shape[0]), 1)
    total = shared_ref[...].astype(jnp.float32)
    for k in range(top):
        chosen = (places == slot_ref[:, k : k + 1]).astype(jnp.float32).astype(jnp.bfloat16)
        picked = jnp.dot(chosen, returned, preferred_element_type=jnp.float32)
        total = total + picked * weight_ref[:, k : k + 1]
    out_ref[...] = total.astype(jnp.bfloat16)


def combine(slot_ids, route_weight, returned, shared):
    tokens, width = shared.shape
    top = slot_ids.shape[1]
    cols = width // 2
    return pl.pallas_call(
        combine_kernel,
        grid=(width // cols,),
        out_shape=jax.ShapeDtypeStruct((tokens, width), jnp.bfloat16),
        in_specs=[
            pl.BlockSpec((tokens, top), lambda i: (0, 0)),
            pl.BlockSpec((tokens, top), lambda i: (0, 0)),
            pl.BlockSpec((tokens, cols), lambda i: (0, i)),
        ]
        + [pl.BlockSpec((chunk.shape[0], cols), lambda i: (0, i)) for chunk in returned],
        out_specs=pl.BlockSpec((tokens, cols), lambda i: (0, i)),
        name="combine",
    )(slot_ids, route_weight, shared, *returned)


def body(
    mixer_input,
    mixer_gain,
    query_one,
    query_two,
    key_one,
    key_two,
    value_weight,
    lambdas,
    head_gain,
    output_weight,
    expert_input,
    expert_gain,
    routes,
    route_weight,
    expert_gate,
    expert_up,
    expert_down,
    shared_gate,
    shared_up,
    shared_down,
):
    ep_size = lax.axis_size("ep")
    tp_size = lax.axis_size("tp")
    ep_rank = lax.axis_index("ep")
    query_cols = query_one.shape[1]
    key_cols = key_one.shape[1]
    local_kv = key_cols // HEAD
    group = query_cols // key_cols
    experts_local = expert_gate.shape[0]

    gates = tp_blocks(expert_gate, tp_size)
    ups = tp_blocks(expert_up, tp_size)
    downs = tp_blocks(expert_down, tp_size)

    token_rows, model_width = expert_input.shape
    normed_experts = normalize(expert_input, expert_gain)
    expert_count = experts_local * ep_size
    top_count = routes.shape[1]
    capacity = max(2, 5 * token_rows * top_count // (4 * expert_count))
    slot_count = expert_count * capacity
    relative = (routes - ep_rank * experts_local) % expert_count
    flat_routes = relative.reshape(-1)
    onehot = (flat_routes[:, None] == jnp.arange(expert_count, dtype=jnp.int32)[None, :]).astype(
        jnp.int32
    )
    slot_place = jnp.sum((jnp.cumsum(onehot, axis=0) - onehot) * onehot, axis=1)
    slot_ids = (flat_routes * capacity + slot_place).reshape(token_rows, top_count)
    slot_match = jnp.arange(slot_count, dtype=jnp.int32)[:, None, None] == slot_ids[None, :, :]
    select = jnp.any(slot_match, axis=2).astype(jnp.bfloat16)
    outgoing = jnp.dot(select, normed_experts, preferred_element_type=jnp.float32).astype(
        jnp.bfloat16
    )
    outgoing, normed_experts = lax.optimization_barrier((outgoing, normed_experts))
    expert_rows = lax.all_gather(normed_experts, "tp", axis=0, tiled=True)
    span = experts_local * capacity
    received = exchange(
        [outgoing[k * span : (k + 1) * span] for k in range(ep_size)], ep_rank, ep_size, 1
    )

    queries, key_values = project(
        mixer_input, mixer_gain, query_one, query_two, key_one, key_two, value_weight
    )
    if ep_size <= MOST_PERMUTES:
        others = [
            lax.ppermute(key_values, "ep", [(i, i + k) for i in range(ep_size - k)])
            for k in range(1, ep_size)
        ]
    else:
        others = [lax.all_gather(key_values, "ep", axis=0)]
    mixer_part = attention(
        ep_rank, lambdas, queries, key_values, others, head_gain, output_weight, local_kv, group
    )
    mixer_sum = lax.psum_scatter(mixer_part, "tp", scatter_dimension=0, tiled=True)

    shared_gated = jnp.dot(expert_rows, shared_gate, preferred_element_type=jnp.float32)
    shared_lifted = jnp.dot(expert_rows, shared_up, preferred_element_type=jnp.float32)
    shared_hidden = (jax.nn.silu(shared_gated) * shared_lifted).astype(jnp.bfloat16)
    shared_part = jnp.dot(shared_hidden, shared_down, preferred_element_type=jnp.float32)
    shared_sum = lax.psum_scatter(
        shared_part.astype(jnp.bfloat16), "tp", scatter_dimension=0, tiled=True
    )

    slot_rows = stack(received).reshape(ep_size, experts_local, capacity, model_width)
    half = max(1, tp_size // 2)
    order = [0, half] + [k for k in range(1, tp_size) if k != half] if tp_size > 1 else [0]
    results = []
    for e in range(experts_local):
        rows = slot_rows[:, e].reshape(ep_size * capacity, model_width)
        total = None
        for first in range(0, len(order), 2):
            part = order[first : first + 2]
            total = routed_part(
                rows,
                [gates[k][e] for k in part],
                [ups[k][e] for k in part],
                [downs[k][e] for k in part],
                total,
                first + 2 >= len(order),
            )
        results.append(total.reshape(ep_size, 1, capacity, model_width))
    routed = jnp.concatenate(results, axis=1).reshape(ep_size, span, model_width)
    returned = exchange([routed[k] for k in range(ep_size)], ep_rank, ep_size, -1)
    expert_output = combine(slot_ids, route_weight, returned, shared_sum)
    return (mixer_sum, expert_output)


def solution(mesh):
    in_specs = (
        P("ep", None),
        P(),
        P(None, "tp"),
        P(None, "tp"),
        P(None, "tp"),
        P(None, "tp"),
        P(None, "tp"),
        P("tp"),
        P(),
        P("tp", None),
        P(("ep", "tp"), None),
        P(),
        P(("ep", "tp"), None),
        P(("ep", "tp"), None),
        P("ep", None, "tp"),
        P("ep", None, "tp"),
        P("ep", "tp", None),
        P(None, "tp"),
        P(None, "tp"),
        P("tp", None),
    )
    out_specs = (P(("ep", "tp"), None), P(("ep", "tp"), None))

    return jax.shard_map(body, mesh=mesh, in_specs=in_specs, out_specs=out_specs, check_vma=False)
```

profile of v0, /device:TPU:0, one launch (start us, length us, event | category | flops | bytes accessed | tf_op | source)
XLA Modules:
  0.0 239.4 jit_solution(14180222198886683830)
XLA Ops:
  7.2 0.7 broadcast_compare_fusion
  8.0 0.1 copy.45
  8.1 0.1 copy.48
  8.2 0.1 eq.44
  8.4 0.1 eq.40
  8.5 0.6 reduce-window.6
  9.1 0.2 slice_reduce_fusion
  9.4 0.1 fusion.13
  9.5 0.1 reduce_sum.21
  9.8 1.3 fusion.1
  11.1 1.2 fusion.3
  12.3 1.6 convolution_convert_fusion.1
  14.0 25.4 %all-gather.2.cloned.1.call-done = bf16[512,2048]{1,0:T(8,128)(2,1)} async-done(((bf16[128,2048]{1,0:T(8,128)(2,1)}), bf16[512,2048]{1,0:T(8,128)(2,1)}) %all-gather.2.cloned.1.call-update) | async-done | bytes 2097168 | tf_op jit(solution)/shard_map/all_gather | solution.py:346
  39.4 2.4 %fusion.18 = f32[512,128]{1,0:T(8,128)S(1)} fusion(bf16[512,2048]{1,0:T(8,128)(2,1)} %all-gather.2.cloned.1.call-done, bf16[2048,128]{1,0:T(8,128)(2,1)S(1)} %copy-done.9), kind=kOutput, calls=%fused_computation.35 | convolution fusion | flops 268435456 | bytes 2883584 | tf_op jit(solution)/shard_map/dot_general | solution.py:367
  41.9 4.7 %convolution_convert_fusion = bf16[512,2048]{1,0:T(8,128)(2,1)} fusion(bf16[128,2048]{1,0:T(8,128)(2,1)S(1)} %copy-done, bf16[512,2048]{1,0:T(8,128)(2,1)S(1)} %copy-done.6, bf16[2048,128]{1,0:T(8,128)(2,1)} %param.38, f32[512,128]{1,0:T(8,128)S(1)} %fusion.18), kind=kOutput, calls=%fused_computation | convolution fusion | flops 538312704 | bytes 5505024 | tf_op jit(solution)/shard_map/dot_general | solution.py:370
  46.7 4.3 %project.1 = (bf16[256,256]{1,0:T(8,128)(2,1)}, bf16[256,256]{1,0:T(8,128)(2,1)}) custom-call(bf16[256,2048]{1,0:T(8,128)(2,1)} %rows_ref.1, f32[1,2048]{1,0:T(1,128)} %bitcast.41, bf16[2048,128]{1,0:T(8,128)(2,1)} %one.1, bf16[2048,128]{1,0:T(8,128)(2,1)} %two.1, bf16[64,2048]{1,0:T(8,128)(2,1)} %bitcast.39, bf16[64,2048]{1,0:T(8,128)(2,1)} %bitcast.40, ...), custom_call_target="tpu_custom_call" | custom-call | flops 2000000000 | bytes 4000000 | tf_op jit(solution)/shard_map/project/pallas_call | solution.py:63
  50.9 3.5 %collective-permute-start = (bf16[256,256]{1,0:T(8,128)(2,1)}, bf16[256,256]{1,0:T(8,128)(2,1)S(1)}, u32[]{:S(2)}, u32[]{:S(2)}) collective-permute-start(bf16[256,256]{1,0:T(8,128)(2,1)} %get-tuple-element.7.refs_3_), channel_id=1, source_target_pairs={{0,4},{4,8},{8,12},{12,16},{16,20},{20,24},{24,28},{1,5},{5,9},{9,... | collective-permute-start | bytes 393224 | tf_op jit(solution)/shard_map/ppermute | solution.py:357
  54.4 3.4 %collective-permute-start.1 = (bf16[256,256]{1,0:T(8,128)(2,1)}, bf16[256,256]{1,0:T(8,128)(2,1)S(1)}, u32[]{:S(2)}, u32[]{:S(2)}) collective-permute-start(bf16[256,256]{1,0:T(8,128)(2,1)} %get-tuple-element.7.refs_3_), channel_id=1, source_target_pairs={{0,8},{4,12},{8,16},{12,20},{16,24},{20,28},{1,9},{5,13},{9,17},{1... | collective-permute-start | bytes 393224 | tf_op jit(solution)/shard_map/ppermute | solution.py:357
  57.8 4.3 %collective-permute-start.2 = (bf16[256,256]{1,0:T(8,128)(2,1)}, bf16[256,256]{1,0:T(8,128)(2,1)S(1)}, u32[]{:S(2)}, u32[]{:S(2)}) collective-permute-start(bf16[256,256]{1,0:T(8,128)(2,1)} %get-tuple-element.7.refs_3_), channel_id=1, source_target_pairs={{0,12},{4,16},{8,20},{12,24},{16,28},{1,13},{5,17},{9,21},{13,25},... | collective-permute-start | bytes 393224 | tf_op jit(solution)/shard_map/ppermute | solution.py:357
  62.2 1.9 collective-permute-start.3
  64.1 1.3 collective-permute-start.4
  65.4 1.3 collective-permute-start.5
  66.7 0.6 copy-done.26
  67.4 1.3 collective-permute-start.6
  68.7 2.2 fusion.17
  71.0 0.1 collective-permute-start.20
  71.0 0.5 collective-permute-done.4.refs_10_
  71.6 0.6 collective-permute-start.16
  72.1 2.2 collective-permute-done.5.refs_11_
  74.4 0.6 collective-permute-start.18
  74.9 2.3 collective-permute-done.6.refs_12_
  77.2 0.6 collective-permute-start.14
  77.7 2.0 collective-permute-done.10.refs_4_
  79.7 1.5 collective-permute-start.11
  81.3 9.8 %collective-permute-done.11.refs_5_ = bf16[40,2048]{1,0:T(8,128)(2,1)S(1)} collective-permute-done((bf16[40,2048]{1,0:T(8,128)(2,1)S(1)}, bf16[40,2048]{1,0:T(8,128)(2,1)S(1)}, u32[]{:S(2)}, u32[]{:S(2)}) %collective-permute-start.11) | collective-permute-done | bytes 163872 | tf_op jit(solution)/shard_map/ppermute | solution.py:22
  91.1 12.4 %collective-permute-start.12 = (bf16[40,2048]{1,0:T(8,128)(2,1)S(1)}, bf16[40,2048]{1,0:T(8,128)(2,1)S(1)}, u32[]{:S(2)}, u32[]{:S(2)}) collective-permute-start(bf16[40,2048]{1,0:T(8,128)(2,1)S(1)} %get-tuple-element.21), channel_id=1, source_target_pairs={{0,24},{4,28},{8,0},{12,4},{16,8},{20,12},{24,16},{28,20},{1,25},{... | collective-permute-start | bytes 491528 | tf_op jit(solution)/shard_map/ppermute | solution.py:22
  103.4 3.4 %collective-permute-done.12.refs_6_ = bf16[40,2048]{1,0:T(8,128)(2,1)S(1)} collective-permute-done((bf16[40,2048]{1,0:T(8,128)(2,1)S(1)}, bf16[40,2048]{1,0:T(8,128)(2,1)S(1)}, u32[]{:S(2)}, u32[]{:S(2)}) %collective-permute-start.12) | collective-permute-done | bytes 163872 | tf_op jit(solution)/shard_map/ppermute | solution.py:22
  106.9 3.8 %collective-permute-start.13 = (bf16[40,2048]{1,0:T(8,128)(2,1)S(1)}, bf16[40,2048]{1,0:T(8,128)(2,1)S(1)}, u32[]{:S(2)}, u32[]{:S(2)}) collective-permute-start(bf16[40,2048]{1,0:T(8,128)(2,1)S(1)} %get-tuple-element.20), channel_id=1, source_target_pairs={{0,28},{4,0},{8,4},{12,8},{16,12},{20,16},{24,20},{28,24},{1,29},{... | collective-permute-start | bytes 491528 | tf_op jit(solution)/shard_map/ppermute | solution.py:22
  110.7 2.8 %collective-permute-done.13.refs_7_ = bf16[40,2048]{1,0:T(8,128)(2,1)S(1)} collective-permute-done((bf16[40,2048]{1,0:T(8,128)(2,1)S(1)}, bf16[40,2048]{1,0:T(8,128)(2,1)S(1)}, u32[]{:S(2)}, u32[]{:S(2)}) %collective-permute-start.13) | collective-permute-done | bytes 163872 | tf_op jit(solution)/shard_map/ppermute | solution.py:22
  113.5 10.2 %collective-permute-done.7.refs_1_ = bf16[40,2048]{1,0:T(8,128)(2,1)S(1)} collective-permute-done((bf16[40,2048]{1,0:T(8,128)(2,1)S(1)}, bf16[40,2048]{1,0:T(8,128)(2,1)S(1)}, u32[]{:S(2)}, u32[]{:S(2)}) %collective-permute-start.7) | collective-permute-done | bytes 163872 | tf_op jit(solution)/shard_map/ppermute | solution.py:22
  123.7 7.6 %collective-permute-done.8.refs_2_ = bf16[40,2048]{1,0:T(8,128)(2,1)S(1)} collective-permute-done((bf16[40,2048]{1,0:T(8,128)(2,1)S(1)}, bf16[40,2048]{1,0:T(8,128)(2,1)S(1)}, u32[]{:S(2)}, u32[]{:S(2)}) %collective-permute-start.8) | collective-permute-done | bytes 163872 | tf_op jit(solution)/shard_map/ppermute | solution.py:22
  131.3 7.1 %collective-permute-done.9.refs_3_ = bf16[40,2048]{1,0:T(8,128)(2,1)S(1)} collective-permute-done((bf16[40,2048]{1,0:T(8,128)(2,1)S(1)}, bf16[40,2048]{1,0:T(8,128)(2,1)S(1)}, u32[]{:S(2)}, u32[]{:S(2)}) %collective-permute-start.9) | collective-permute-done | bytes 163872 | tf_op jit(solution)/shard_map/ppermute | solution.py:22
  138.5 1.0 copy-done.4
  139.5 0.5 collective-permute-start.22
  140.0 0.5 collective-permute-start.19
  140.5 3.7 %collective-permute-done.14 = bf16[1,2048,256]{2,1,0:T(8,128)(2,1)} collective-permute-done((bf16[1,2048,256]{2,1,0:T(8,128)(2,1)S(1)}, bf16[1,2048,256]{2,1,0:T(8,128)(2,1)}, u32[]{:S(2)}, u32[]{:S(2)}) %collective-permute-start.14) | collective-permute-done | bytes 1048608 | tf_op jit(solution)/shard_map/ppermute | solution.py:136
  144.3 4.3 %attention.1 = bf16[256,2048]{1,0:T(8,128)(2,1)} custom-call(s32[1]{0:T(128)} %bitcast.refs_0_, f32[2]{0:T(128)} %refs_1_.1, bf16[256,256]{1,0:T(8,128)(2,1)} %get-tuple-element.6.refs_2_, bf16[256,256]{1,0:T(8,128)(2,1)} %get-tuple-element.7.refs_3_, f32[1,128]{1,0:T(1,128)} %bitcast.42, bf16[256,2048]{1,0:T(8,128)(2,1)} %refs_5_.1, ...), custom_call_target="tpu_custom_call" | custom-call | flops 6000000000 | bytes 4000000 | tf_op jit(solution)/shard_map/attention/pallas_call | solution.py:243
  148.7 2.6 %stack.1 = bf16[8,40,2048]{2,1,0:T(8,128)(2,1)} custom-call(bf16[40,2048]{1,0:T(8,128)(2,1)} %get-tuple-element.27.refs_0_, bf16[40,2048]{1,0:T(8,128)(2,1)} %copy-done.14, bf16[40,2048]{1,0:T(8,128)(2,1)} %copy-done.15, bf16[40,2048]{1,0:T(8,128)(2,1)} %copy-done.16, bf16[40,2048]{1,0:T(8,128)(2,1)} %copy-done.10, bf16[40,2048]{1,0:T(8,128)(2,1)} %copy-done.11, ...), custom_call_target="tpu_custom_call" | custom-call | tf_op jit(solution)/shard_map/stack/pallas_call | solution.py:87
  151.3 1.2 copy-done.3
  152.5 1.2 copy-done.5
  153.7 5.6 %routed.2.refs_7_ = f32[320,2048]{1,0:T(8,128)} custom-call(bf16[320,2048]{1,0:T(8,128)(2,1)} %bitcast.37, bf16[2048,256]{1,0:T(8,128)(2,1)S(1)} %bitcast.33, bf16[2048,256]{1,0:T(8,128)(2,1)S(1)} %bitcast.36, bf16[2048,256]{1,0:T(8,128)(2,1)S(1)} %bitcast.34, bf16[2048,256]{1,0:T(8,128)(2,1)} %bitcast.17.refs_4_, bf16[256,2048]{1,0:T(8,128)(2,1)S(1)} %bitcast.35, ...), custom_call_target="tpu_custom_call" | custom-call | flops 4000000000 | bytes 8000000 | tf_op jit(solution)/shard_map/routed/pallas_call | solution.py:118
  159.4 7.3 %routed.3 = bf16[320,2048]{1,0:T(8,128)(2,1)} custom-call(bf16[320,2048]{1,0:T(8,128)(2,1)} %bitcast.38, bf16[2048,256]{1,0:T(8,128)(2,1)} %bitcast.8.refs_1_, bf16[2048,256]{1,0:T(8,128)(2,1)} %bitcast.9.refs_2_, bf16[2048,256]{1,0:T(8,128)(2,1)} %bitcast.10.refs_3_, bf16[2048,256]{1,0:T(8,128)(2,1)} %bitcast.11.refs_4_, ...), custom_call_target="tpu_custom_call" | custom-call | flops 4000000000 | bytes 8000000 | tf_op jit(solution)/shard_map/routed/pallas_call | solution.py:118
  166.7 2.2 fusion.16
  168.9 30.8 %collective-permute-start.23 = (bf16[40,2048]{1,0:T(8,128)(2,1)S(1)}, bf16[40,2048]{1,0:T(8,128)(2,1)S(1)}, u32[]{:S(2)}, u32[]{:S(2)}) collective-permute-start(bf16[40,2048]{1,0:T(8,128)(2,1)S(1)} %get-tuple-element.18), channel_id=1, source_target_pairs={{0,28},{4,0},{8,4},{12,8},{16,12},{20,16},{24,20},{28,24},{1,29},{... | collective-permute-start | bytes 491528 | tf_op jit(solution)/shard_map/ppermute | solution.py:22
  199.6 2.9 %collective-permute-start.26 = (bf16[40,2048]{1,0:T(8,128)(2,1)S(1)}, bf16[40,2048]{1,0:T(8,128)(2,1)S(1)}, u32[]{:S(2)}, u32[]{:S(2)}) collective-permute-start(bf16[40,2048]{1,0:T(8,128)(2,1)S(1)} %get-tuple-element.15), channel_id=1, source_target_pairs={{0,16},{4,20},{8,24},{12,28},{16,0},{20,4},{24,8},{28,12},{1,17},{... | collective-permute-start | bytes 491528 | tf_op jit(solution)/shard_map/ppermute | solution.py:22
  202.6 1.7 collective-permute-done.23.rest_1_
  204.3 0.3 collective-permute-start.28
  204.6 3.2 %collective-permute-done.24.rest_2_ = bf16[40,2048]{1,0:T(8,128)(2,1)S(1)} collective-permute-done((bf16[40,2048]{1,0:T(8,128)(2,1)S(1)}, bf16[40,2048]{1,0:T(8,128)(2,1)S(1)}, u32[]{:S(2)}, u32[]{:S(2)}) %collective-permute-start.24) | collective-permute-done | bytes 163872 | tf_op jit(solution)/shard_map/ppermute | solution.py:22
  207.8 0.7 copy.50.weight_ref
  208.6 2.8 %collective-permute-done.25.rest_3_ = bf16[40,2048]{1,0:T(8,128)(2,1)S(1)} collective-permute-done((bf16[40,2048]{1,0:T(8,128)(2,1)S(1)}, bf16[40,2048]{1,0:T(8,128)(2,1)S(1)}, u32[]{:S(2)}, u32[]{:S(2)}) %collective-permute-start.25) | collective-permute-done | bytes 163872 | tf_op jit(solution)/shard_map/ppermute | solution.py:22
  211.4 12.9 %collective-permute-done.26.rest_4_ = bf16[40,2048]{1,0:T(8,128)(2,1)S(1)} collective-permute-done((bf16[40,2048]{1,0:T(8,128)(2,1)S(1)}, bf16[40,2048]{1,0:T(8,128)(2,1)S(1)}, u32[]{:S(2)}, u32[]{:S(2)}) %collective-permute-start.26) | collective-permute-done | bytes 163872 | tf_op jit(solution)/shard_map/ppermute | solution.py:22
  224.3 4.6 %collective-permute-done.27.rest_5_ = bf16[40,2048]{1,0:T(8,128)(2,1)S(1)} collective-permute-done((bf16[40,2048]{1,0:T(8,128)(2,1)S(1)}, bf16[40,2048]{1,0:T(8,128)(2,1)S(1)}, u32[]{:S(2)}, u32[]{:S(2)}) %collective-permute-start.27) | collective-permute-done | bytes 163872 | tf_op jit(solution)/shard_map/ppermute | solution.py:22
  229.1 0.6 copy-done.21
  229.8 3.0 %combine.1 = bf16[128,2048]{1,0:T(8,128)(2,1)} custom-call(s32[128,2]{1,0:T(8,128)} %copy-done.8, f32[128,2]{1,0:T(8,128)} %copy.50.weight_ref, bf16[128,2048]{1,0:T(8,128)(2,1)} %reduce-scatter.5.cloned.1.call-done.shared_ref, bf16[40,2048]{1,0:T(8,128)(2,1)} %get-tuple-element.19.rest_0_, bf16[40,2048]{1,0:T(8,128)(2,1)} %copy-done.17, ...), custom_call_target="tpu_custom_call" | custom-call | tf_op jit(solution)/shard_map/combine/pallas_call | solution.py:277
  (100 shorter events, 0.8 us)
Async XLA Ops:
  7.2 34.7 %copy-start = (bf16[128,2048]{1,0:T(8,128)(2,1)S(1)}, bf16[128,2048]{1,0:T(8,128)(2,1)}, u32[]{:S(2)}) copy-start(bf16[128,2048]{1,0:T(8,128)(2,1)} %param.39) | copy-start | bytes 1572868
  7.2 32.2 %all-gather.2.cloned.1.call-start = ((), (), s32[]{:S(2)}) async-start(), calls=%async_computation.3 | async-start | bytes 2621440 | tf_op jit(solution)/shard_map/all_gather | solution.py:346
  9.6 32.2 %copy-start.8 = (s32[128,2]{1,0:T(8,128)}, s32[128,2]{1,0:T(8,128)S(1)}, u32[]{:S(2)}) copy-start(s32[128,2]{1,0:T(8,128)S(1)} %multiply_add_fusion.slot_ref) | copy-start | bytes 3076
  9.7 29.7 %copy-start.9 = (bf16[2048,128]{1,0:T(8,128)(2,1)S(1)}, bf16[2048,128]{1,0:T(8,128)(2,1)}, u32[]{:S(2)}) copy-start(bf16[2048,128]{1,0:T(8,128)(2,1)} %param.37) | copy-start | bytes 1572868
  12.3 1.6 copy-start.7
  13.9 215.1 %reduce-scatter.5.cloned.1.call-start = ((), (), s32[]{:S(2)}) async-start(), calls=%async_computation.4 | async-start | bytes 2621440 | tf_op jit(solution)/shard_map/reduce_scatter | solution.py:371
  39.4 2.5 %copy-start.6 = (bf16[512,2048]{1,0:T(8,128)(2,1)S(1)}, bf16[512,2048]{1,0:T(8,128)(2,1)}, u32[]{:S(2)}) copy-start(bf16[512,2048]{1,0:T(8,128)(2,1)} %all-gather.2.cloned.1.call-done) | copy-start | bytes 6291460
  46.6 186.2 %reduce-scatter.3.cloned.1.call-start = ((), (), s32[]{:S(2)}) async-start(), calls=%async_computation.2 | async-start | bytes 1310720 | tf_op jit(solution)/shard_map/reduce_scatter | solution.py:365
  50.9 20.0 %copy-start.1 = (bf16[1,2048,256]{2,1,0:T(8,128)(2,1)S(1)}, bf16[1,2048,256]{2,1,0:T(8,128)(2,1)}, u32[]{:S(2)}) copy-start(bf16[1,2048,256]{2,1,0:T(8,128)(2,1)} %param.34) | copy-start | bytes 3145732
  50.9 20.6 %copy-start.2 = (bf16[1,2048,256]{2,1,0:T(8,128)(2,1)S(1)}, bf16[1,2048,256]{2,1,0:T(8,128)(2,1)}, u32[]{:S(2)}) copy-start(bf16[1,2048,256]{2,1,0:T(8,128)(2,1)} %param.35) | copy-start | bytes 3145732
  50.9 14.5 %collective-permute-start = (bf16[256,256]{1,0:T(8,128)(2,1)}, bf16[256,256]{1,0:T(8,128)(2,1)S(1)}, u32[]{:S(2)}, u32[]{:S(2)}) collective-permute-start(bf16[256,256]{1,0:T(8,128)(2,1)} %get-tuple-element.7.refs_3_), channel_id=1, source_target_pairs={{0,4},{4,8},{8,12},{12,16},{16,20},{20,24},{24,28},{1,5},{5,9},{9,... | collective-permute-start | bytes 393224 | tf_op jit(solution)/shard_map/ppermute | solution.py:357
  54.4 12.3 %collective-permute-start.1 = (bf16[256,256]{1,0:T(8,128)(2,1)}, bf16[256,256]{1,0:T(8,128)(2,1)S(1)}, u32[]{:S(2)}, u32[]{:S(2)}) collective-permute-start(bf16[256,256]{1,0:T(8,128)(2,1)} %get-tuple-element.7.refs_3_), channel_id=1, source_target_pairs={{0,8},{4,12},{8,16},{12,20},{16,24},{20,28},{1,9},{5,13},{9,17},{1... | collective-permute-start | bytes 393224 | tf_op jit(solution)/shard_map/ppermute | solution.py:357
  57.8 13.0 %collective-permute-start.2 = (bf16[256,256]{1,0:T(8,128)(2,1)}, bf16[256,256]{1,0:T(8,128)(2,1)S(1)}, u32[]{:S(2)}, u32[]{:S(2)}) collective-permute-start(bf16[256,256]{1,0:T(8,128)(2,1)} %get-tuple-element.7.refs_3_), channel_id=1, source_target_pairs={{0,12},{4,16},{8,20},{12,24},{16,28},{1,13},{5,17},{9,21},{13,25},... | collective-permute-start | bytes 393224 | tf_op jit(solution)/shard_map/ppermute | solution.py:357
  62.2 8.8 %collective-permute-start.3 = (bf16[256,256]{1,0:T(8,128)(2,1)}, bf16[256,256]{1,0:T(8,128)(2,1)S(1)}, u32[]{:S(2)}, u32[]{:S(2)}) collective-permute-start(bf16[256,256]{1,0:T(8,128)(2,1)} %get-tuple-element.7.refs_3_), channel_id=1, source_target_pairs={{0,16},{4,20},{8,24},{12,28},{1,17},{5,21},{9,25},{13,29},{2,18},{... | collective-permute-start | bytes 393224 | tf_op jit(solution)/shard_map/ppermute | solution.py:357
  64.1 7.5 %collective-permute-start.4 = (bf16[256,256]{1,0:T(8,128)(2,1)}, bf16[256,256]{1,0:T(8,128)(2,1)S(1)}, u32[]{:S(2)}, u32[]{:S(2)}) collective-permute-start(bf16[256,256]{1,0:T(8,128)(2,1)} %get-tuple-element.7.refs_3_), channel_id=1, source_target_pairs={{0,20},{4,24},{8,28},{1,21},{5,25},{9,29},{2,22},{6,26},{10,30},{3... | collective-permute-start | bytes 393224 | tf_op jit(solution)/shard_map/ppermute | solution.py:357
  65.4 1.3 copy-start.25
  65.4 9.0 %collective-permute-start.5 = (bf16[256,256]{1,0:T(8,128)(2,1)}, bf16[256,256]{1,0:T(8,128)(2,1)S(1)}, u32[]{:S(2)}, u32[]{:S(2)}) collective-permute-start(bf16[256,256]{1,0:T(8,128)(2,1)} %get-tuple-element.7.refs_3_), channel_id=1, source_target_pairs={{0,24},{4,28},{1,25},{5,29},{2,26},{6,30},{3,27},{7,31}} | collective-permute-start | bytes 393224 | tf_op jit(solution)/shard_map/ppermute | solution.py:357
  67.4 9.8 %collective-permute-start.6 = (bf16[256,256]{1,0:T(8,128)(2,1)}, bf16[256,256]{1,0:T(8,128)(2,1)S(1)}, u32[]{:S(2)}, u32[]{:S(2)}) collective-permute-start(bf16[256,256]{1,0:T(8,128)(2,1)} %get-tuple-element.7.refs_3_), channel_id=1, source_target_pairs={{0,28},{1,29},{2,30},{3,31}} | collective-permute-start | bytes 393224 | tf_op jit(solution)/shard_map/ppermute | solution.py:357
  70.8 73.4 %copy-start.27 = (bf16[256,256]{1,0:T(8,128)(2,1)}, bf16[256,256]{1,0:T(8,128)(2,1)S(1)}, u32[]{:S(2)}) copy-start(bf16[256,256]{1,0:T(8,128)(2,1)S(1)} %collective-permute-done.2.refs_8_) | copy-start | bytes 393220
  70.9 8.9 %collective-permute-start.10 = (bf16[40,2048]{1,0:T(8,128)(2,1)S(1)}, bf16[40,2048]{1,0:T(8,128)(2,1)S(1)}, u32[]{:S(2)}, u32[]{:S(2)}) collective-permute-start(bf16[40,2048]{1,0:T(8,128)(2,1)S(1)} %get-tuple-element.23), channel_id=1, source_target_pairs={{0,16},{4,20},{8,24},{12,28},{16,0},{20,4},{24,8},{28,12},{1,17},{... | collective-permute-start | bytes 491528 | tf_op jit(solution)/shard_map/ppermute | solution.py:22
  70.9 73.3 %copy-start.28 = (bf16[256,256]{1,0:T(8,128)(2,1)}, bf16[256,256]{1,0:T(8,128)(2,1)S(1)}, u32[]{:S(2)}) copy-start(bf16[256,256]{1,0:T(8,128)(2,1)S(1)} %collective-permute-done.3.refs_9_) | copy-start | bytes 393220
  71.0 67.5 %collective-permute-start.20 = (bf16[1,2048,256]{2,1,0:T(8,128)(2,1)S(1)}, bf16[1,2048,256]{2,1,0:T(8,128)(2,1)S(1)}, u32[]{:S(2)}, u32[]{:S(2)}) collective-permute-start(bf16[1,2048,256]{2,1,0:T(8,128)(2,1)S(1)} %copy-done.1), channel_id=1, source_target_pairs={{0,1},{1,0},{2,3},{3,2},{4,5},{5,4},{6,7},{7,6},{8,9},{9,8},{10,11... | collective-permute-start | bytes 3145736 | tf_op jit(solution)/shard_map/ppermute | solution.py:136
  71.6 72.7 %copy-start.29 = (bf16[256,256]{1,0:T(8,128)(2,1)}, bf16[256,256]{1,0:T(8,128)(2,1)S(1)}, u32[]{:S(2)}) copy-start(bf16[256,256]{1,0:T(8,128)(2,1)S(1)} %collective-permute-done.4.refs_10_) | copy-start | bytes 393220
  71.6 68.4 %collective-permute-start.16 = (bf16[1,2048,256]{2,1,0:T(8,128)(2,1)S(1)}, bf16[1,2048,256]{2,1,0:T(8,128)(2,1)}, u32[]{:S(2)}, u32[]{:S(2)}) collective-permute-start(bf16[1,2048,256]{2,1,0:T(8,128)(2,1)S(1)} %copy-done.2), channel_id=1, source_target_pairs={{0,2},{1,3},{2,0},{3,1},{4,6},{5,7},{6,4},{7,5},{8,10},{9,11},{10,... | collective-permute-start | bytes 3145736 | tf_op jit(solution)/shard_map/ppermute | solution.py:136
  74.4 69.9 %copy-start.30 = (bf16[256,256]{1,0:T(8,128)(2,1)}, bf16[256,256]{1,0:T(8,128)(2,1)S(1)}, u32[]{:S(2)}) copy-start(bf16[256,256]{1,0:T(8,128)(2,1)S(1)} %collective-permute-done.5.refs_11_) | copy-start | bytes 393220
  74.4 65.6 %collective-permute-start.18 = (bf16[1,256,2048]{2,1,0:T(8,128)(2,1)}, bf16[1,256,2048]{2,1,0:T(8,128)(2,1)}, u32[]{:S(2)}, u32[]{:S(2)}) collective-permute-start(bf16[1,256,2048]{2,1,0:T(8,128)(2,1)} %param.36), channel_id=1, source_target_pairs={{0,2},{1,3},{2,0},{3,1},{4,6},{5,7},{6,4},{7,5},{8,10},{9,11},{10,... | collective-permute-start | bytes 3145736 | tf_op jit(solution)/shard_map/ppermute | solution.py:136
  77.2 67.1 %copy-start.31 = (bf16[256,256]{1,0:T(8,128)(2,1)}, bf16[256,256]{1,0:T(8,128)(2,1)S(1)}, u32[]{:S(2)}) copy-start(bf16[256,256]{1,0:T(8,128)(2,1)S(1)} %collective-permute-done.6.refs_12_) | copy-start | bytes 393220
  77.2 67.0 %collective-permute-start.14 = (bf16[1,2048,256]{2,1,0:T(8,128)(2,1)S(1)}, bf16[1,2048,256]{2,1,0:T(8,128)(2,1)}, u32[]{:S(2)}, u32[]{:S(2)}) collective-permute-start(bf16[1,2048,256]{2,1,0:T(8,128)(2,1)S(1)} %copy-done.1), channel_id=1, source_target_pairs={{0,2},{1,3},{2,0},{3,1},{4,6},{5,7},{6,4},{7,5},{8,10},{9,11},{10,... | collective-permute-start | bytes 3145736 | tf_op jit(solution)/shard_map/ppermute | solution.py:136
  79.7 68.9 %copy-start.10 = (bf16[40,2048]{1,0:T(8,128)(2,1)}, bf16[40,2048]{1,0:T(8,128)(2,1)S(1)}, u32[]{:S(2)}) copy-start(bf16[40,2048]{1,0:T(8,128)(2,1)S(1)} %collective-permute-done.10.refs_4_) | copy-start | bytes 491524
  79.7 11.3 %collective-permute-start.11 = (bf16[40,2048]{1,0:T(8,128)(2,1)S(1)}, bf16[40,2048]{1,0:T(8,128)(2,1)S(1)}, u32[]{:S(2)}, u32[]{:S(2)}) collective-permute-start(bf16[40,2048]{1,0:T(8,128)(2,1)S(1)} %get-tuple-element.22), channel_id=1, source_target_pairs={{0,20},{4,24},{8,28},{12,0},{16,4},{20,8},{24,12},{28,16},{1,21},{... | collective-permute-start | bytes 491528 | tf_op jit(solution)/shard_map/ppermute | solution.py:22
  91.1 57.6 %copy-start.11 = (bf16[40,2048]{1,0:T(8,128)(2,1)}, bf16[40,2048]{1,0:T(8,128)(2,1)S(1)}, u32[]{:S(2)}) copy-start(bf16[40,2048]{1,0:T(8,128)(2,1)S(1)} %collective-permute-done.11.refs_5_) | copy-start | bytes 491524
  91.1 15.8 %collective-permute-start.12 = (bf16[40,2048]{1,0:T(8,128)(2,1)S(1)}, bf16[40,2048]{1,0:T(8,128)(2,1)S(1)}, u32[]{:S(2)}, u32[]{:S(2)}) collective-permute-start(bf16[40,2048]{1,0:T(8,128)(2,1)S(1)} %get-tuple-element.21), channel_id=1, source_target_pairs={{0,24},{4,28},{8,0},{12,4},{16,8},{20,12},{24,16},{28,20},{1,25},{... | collective-permute-start | bytes 491528 | tf_op jit(solution)/shard_map/ppermute | solution.py:22
  106.9 41.8 %copy-start.12 = (bf16[40,2048]{1,0:T(8,128)(2,1)}, bf16[40,2048]{1,0:T(8,128)(2,1)S(1)}, u32[]{:S(2)}) copy-start(bf16[40,2048]{1,0:T(8,128)(2,1)S(1)} %collective-permute-done.12.refs_6_) | copy-start | bytes 491524
  106.9 6.7 %collective-permute-start.13 = (bf16[40,2048]{1,0:T(8,128)(2,1)S(1)}, bf16[40,2048]{1,0:T(8,128)(2,1)S(1)}, u32[]{:S(2)}, u32[]{:S(2)}) collective-permute-start(bf16[40,2048]{1,0:T(8,128)(2,1)S(1)} %get-tuple-element.20), channel_id=1, source_target_pairs={{0,28},{4,0},{8,4},{12,8},{16,12},{20,16},{24,20},{28,24},{1,29},{... | collective-permute-start | bytes 491528 | tf_op jit(solution)/shard_map/ppermute | solution.py:22
  113.5 35.1 %copy-start.13 = (bf16[40,2048]{1,0:T(8,128)(2,1)}, bf16[40,2048]{1,0:T(8,128)(2,1)S(1)}, u32[]{:S(2)}) copy-start(bf16[40,2048]{1,0:T(8,128)(2,1)S(1)} %collective-permute-done.13.refs_7_) | copy-start | bytes 491524
  113.5 10.2 %collective-permute-start.7 = (bf16[40,2048]{1,0:T(8,128)(2,1)S(1)}, bf16[40,2048]{1,0:T(8,128)(2,1)S(1)}, u32[]{:S(2)}, u32[]{:S(2)}) collective-permute-start(bf16[40,2048]{1,0:T(8,128)(2,1)S(1)} %get-tuple-element.26), channel_id=1, source_target_pairs={{0,4},{4,8},{8,12},{12,16},{16,20},{20,24},{24,28},{28,0},{1,5},{5... | collective-permute-start | bytes 491528 | tf_op jit(solution)/shard_map/ppermute | solution.py:22
  123.7 24.9 %copy-start.14 = (bf16[40,2048]{1,0:T(8,128)(2,1)}, bf16[40,2048]{1,0:T(8,128)(2,1)S(1)}, u32[]{:S(2)}) copy-start(bf16[40,2048]{1,0:T(8,128)(2,1)S(1)} %collective-permute-done.7.refs_1_) | copy-start | bytes 491524
  123.7 7.6 %collective-permute-start.8 = (bf16[40,2048]{1,0:T(8,128)(2,1)S(1)}, bf16[40,2048]{1,0:T(8,128)(2,1)S(1)}, u32[]{:S(2)}, u32[]{:S(2)}) collective-permute-start(bf16[40,2048]{1,0:T(8,128)(2,1)S(1)} %get-tuple-element.25), channel_id=1, source_target_pairs={{0,8},{4,12},{8,16},{12,20},{16,24},{20,28},{24,0},{28,4},{1,9},{5... | collective-permute-start | bytes 491528 | tf_op jit(solution)/shard_map/ppermute | solution.py:22
  131.3 12.9 %copy-start.15 = (bf16[40,2048]{1,0:T(8,128)(2,1)}, bf16[40,2048]{1,0:T(8,128)(2,1)S(1)}, u32[]{:S(2)}) copy-start(bf16[40,2048]{1,0:T(8,128)(2,1)S(1)} %collective-permute-done.8.refs_2_) | copy-start | bytes 491524
  131.3 7.1 %collective-permute-start.9 = (bf16[40,2048]{1,0:T(8,128)(2,1)S(1)}, bf16[40,2048]{1,0:T(8,128)(2,1)S(1)}, u32[]{:S(2)}, u32[]{:S(2)}) collective-permute-start(bf16[40,2048]{1,0:T(8,128)(2,1)S(1)} %get-tuple-element.24), channel_id=1, source_target_pairs={{0,12},{4,16},{8,20},{12,24},{16,28},{20,0},{24,4},{28,8},{1,13},{... | collective-permute-start | bytes 491528 | tf_op jit(solution)/shard_map/ppermute | solution.py:22
  138.5 5.8 %copy-start.16 = (bf16[40,2048]{1,0:T(8,128)(2,1)}, bf16[40,2048]{1,0:T(8,128)(2,1)S(1)}, u32[]{:S(2)}) copy-start(bf16[40,2048]{1,0:T(8,128)(2,1)S(1)} %collective-permute-done.9.refs_3_) | copy-start | bytes 491524
  138.5 12.8 %collective-permute-start.21 = (bf16[1,2048,256]{2,1,0:T(8,128)(2,1)S(1)}, bf16[1,2048,256]{2,1,0:T(8,128)(2,1)}, u32[]{:S(2)}, u32[]{:S(2)}) collective-permute-start(bf16[1,2048,256]{2,1,0:T(8,128)(2,1)S(1)} %copy-done.2), channel_id=1, source_target_pairs={{0,1},{1,0},{2,3},{3,2},{4,5},{5,4},{6,7},{7,6},{8,9},{9,8},{10,11... | collective-permute-start | bytes 3145736 | tf_op jit(solution)/shard_map/ppermute | solution.py:136
  138.5 1.0 copy-start.4
  139.5 11.8 %collective-permute-start.22 = (bf16[1,256,2048]{2,1,0:T(8,128)(2,1)}, bf16[1,256,2048]{2,1,0:T(8,128)(2,1)}, u32[]{:S(2)}, u32[]{:S(2)}) collective-permute-start(bf16[1,256,2048]{2,1,0:T(8,128)(2,1)} %param.36), channel_id=1, source_target_pairs={{0,1},{1,0},{2,3},{3,2},{4,5},{5,4},{6,7},{7,6},{8,9},{9,8},{10,11... | collective-permute-start | bytes 3145736 | tf_op jit(solution)/shard_map/ppermute | solution.py:136
  140.0 19.4 %collective-permute-start.17 = (bf16[1,2048,256]{2,1,0:T(8,128)(2,1)}, bf16[1,2048,256]{2,1,0:T(8,128)(2,1)}, u32[]{:S(2)}, u32[]{:S(2)}) collective-permute-start(bf16[1,2048,256]{2,1,0:T(8,128)(2,1)} %collective-permute-done.16), channel_id=1, source_target_pairs={{0,1},{1,0},{2,3},{3,2},{4,5},{5,4},{6,7},{7,6},{8,9},{9,8},{10,11... | collective-permute-start | bytes 3145736 | tf_op jit(solution)/shard_map/ppermute | solution.py:136
  140.0 19.4 %collective-permute-start.19 = (bf16[1,256,2048]{2,1,0:T(8,128)(2,1)}, bf16[1,256,2048]{2,1,0:T(8,128)(2,1)}, u32[]{:S(2)}, u32[]{:S(2)}) collective-permute-start(bf16[1,256,2048]{2,1,0:T(8,128)(2,1)} %collective-permute-done.18), channel_id=1, source_target_pairs={{0,1},{1,0},{2,3},{3,2},{4,5},{5,4},{6,7},{7,6},{8,9},{9,8},{10,11... | collective-permute-start | bytes 3145736 | tf_op jit(solution)/shard_map/ppermute | solution.py:136
  144.2 15.1 %collective-permute-start.15 = (bf16[1,2048,256]{2,1,0:T(8,128)(2,1)}, bf16[1,2048,256]{2,1,0:T(8,128)(2,1)}, u32[]{:S(2)}, u32[]{:S(2)}) collective-permute-start(bf16[1,2048,256]{2,1,0:T(8,128)(2,1)} %collective-permute-done.14), channel_id=1, source_target_pairs={{0,1},{1,0},{2,3},{3,2},{4,5},{5,4},{6,7},{7,6},{8,9},{9,8},{10,11... | collective-permute-start | bytes 3145736 | tf_op jit(solution)/shard_map/ppermute | solution.py:136
  151.3 1.2 copy-start.3
  152.5 1.2 copy-start.5
  166.7 41.1 %copy-start.24 = (f32[128,2]{0,1:T(2,128)S(1)}, f32[128,2]{0,1:T(2,128)}, u32[]{:S(2)}) copy-start(f32[128,2]{0,1:T(2,128)} %param.33) | copy-start | bytes 3076
  168.9 35.4 %collective-permute-start.23 = (bf16[40,2048]{1,0:T(8,128)(2,1)S(1)}, bf16[40,2048]{1,0:T(8,128)(2,1)S(1)}, u32[]{:S(2)}, u32[]{:S(2)}) collective-permute-start(bf16[40,2048]{1,0:T(8,128)(2,1)S(1)} %get-tuple-element.18), channel_id=1, source_target_pairs={{0,28},{4,0},{8,4},{12,8},{16,12},{20,16},{24,20},{28,24},{1,29},{... | collective-permute-start | bytes 491528 | tf_op jit(solution)/shard_map/ppermute | solution.py:22
  199.6 8.2 %collective-permute-start.24 = (bf16[40,2048]{1,0:T(8,128)(2,1)S(1)}, bf16[40,2048]{1,0:T(8,128)(2,1)S(1)}, u32[]{:S(2)}, u32[]{:S(2)}) collective-permute-start(bf16[40,2048]{1,0:T(8,128)(2,1)S(1)} %get-tuple-element.17), channel_id=1, source_target_pairs={{0,24},{4,28},{8,0},{12,4},{16,8},{20,12},{24,16},{28,20},{1,25},{... | collective-permute-start | bytes 491528 | tf_op jit(solution)/shard_map/ppermute | solution.py:22
  199.6 11.7 %collective-permute-start.25 = (bf16[40,2048]{1,0:T(8,128)(2,1)S(1)}, bf16[40,2048]{1,0:T(8,128)(2,1)S(1)}, u32[]{:S(2)}, u32[]{:S(2)}) collective-permute-start(bf16[40,2048]{1,0:T(8,128)(2,1)S(1)} %get-tuple-element.16), channel_id=1, source_target_pairs={{0,20},{4,24},{8,28},{12,0},{16,4},{20,8},{24,12},{28,16},{1,21},{... | collective-permute-start | bytes 491528 | tf_op jit(solution)/shard_map/ppermute | solution.py:22
  199.6 24.7 %collective-permute-start.26 = (bf16[40,2048]{1,0:T(8,128)(2,1)S(1)}, bf16[40,2048]{1,0:T(8,128)(2,1)S(1)}, u32[]{:S(2)}, u32[]{:S(2)}) collective-permute-start(bf16[40,2048]{1,0:T(8,128)(2,1)S(1)} %get-tuple-element.15), channel_id=1, source_target_pairs={{0,16},{4,20},{8,24},{12,28},{16,0},{20,4},{24,8},{28,12},{1,17},{... | collective-permute-start | bytes 491528 | tf_op jit(solution)/shard_map/ppermute | solution.py:22
  202.6 26.4 %collective-permute-start.27 = (bf16[40,2048]{1,0:T(8,128)(2,1)S(1)}, bf16[40,2048]{1,0:T(8,128)(2,1)S(1)}, u32[]{:S(2)}, u32[]{:S(2)}) collective-permute-start(bf16[40,2048]{1,0:T(8,128)(2,1)S(1)} %get-tuple-element.14), channel_id=1, source_target_pairs={{0,12},{4,16},{8,20},{12,24},{16,28},{20,0},{24,4},{28,8},{1,13},{... | collective-permute-start | bytes 491528 | tf_op jit(solution)/shard_map/ppermute | solution.py:22
  204.3 24.8 %copy-start.17 = (bf16[40,2048]{1,0:T(8,128)(2,1)}, bf16[40,2048]{1,0:T(8,128)(2,1)S(1)}, u32[]{:S(2)}) copy-start(bf16[40,2048]{1,0:T(8,128)(2,1)S(1)} %collective-permute-done.23.rest_1_) | copy-start | bytes 491524
  204.3 24.7 %collective-permute-start.28 = (bf16[40,2048]{1,0:T(8,128)(2,1)S(1)}, bf16[40,2048]{1,0:T(8,128)(2,1)S(1)}, u32[]{:S(2)}, u32[]{:S(2)}) collective-permute-start(bf16[40,2048]{1,0:T(8,128)(2,1)S(1)} %get-tuple-element.13), channel_id=1, source_target_pairs={{0,8},{4,12},{8,16},{12,20},{16,24},{20,28},{24,0},{28,4},{1,9},{5... | collective-permute-start | bytes 491528 | tf_op jit(solution)/shard_map/ppermute | solution.py:22
  207.8 21.2 %copy-start.18 = (bf16[40,2048]{1,0:T(8,128)(2,1)}, bf16[40,2048]{1,0:T(8,128)(2,1)S(1)}, u32[]{:S(2)}) copy-start(bf16[40,2048]{1,0:T(8,128)(2,1)S(1)} %collective-permute-done.24.rest_2_) | copy-start | bytes 491524
  207.8 21.2 %collective-permute-start.29 = (bf16[40,2048]{1,0:T(8,128)(2,1)S(1)}, bf16[40,2048]{1,0:T(8,128)(2,1)S(1)}, u32[]{:S(2)}, u32[]{:S(2)}) collective-permute-start(bf16[40,2048]{1,0:T(8,128)(2,1)S(1)} %get-tuple-element.12), channel_id=1, source_target_pairs={{0,4},{4,8},{8,12},{12,16},{16,20},{20,24},{24,28},{28,0},{1,5},{5... | collective-permute-start | bytes 491528 | tf_op jit(solution)/shard_map/ppermute | solution.py:22
  211.4 17.7 %copy-start.19 = (bf16[40,2048]{1,0:T(8,128)(2,1)}, bf16[40,2048]{1,0:T(8,128)(2,1)S(1)}, u32[]{:S(2)}) copy-start(bf16[40,2048]{1,0:T(8,128)(2,1)S(1)} %collective-permute-done.25.rest_3_) | copy-start | bytes 491524
  224.3 4.7 %copy-start.20 = (bf16[40,2048]{1,0:T(8,128)(2,1)}, bf16[40,2048]{1,0:T(8,128)(2,1)S(1)}, u32[]{:S(2)}) copy-start(bf16[40,2048]{1,0:T(8,128)(2,1)S(1)} %collective-permute-done.26.rest_4_) | copy-start | bytes 491524
  229.0 0.7 copy-start.21
  229.0 0.7 copy-start.22
  229.0 0.8 copy-start.23
  (1 other events, 0.6 us)
Sparse Core Ops, SparseCore 0:
  14.1 25.2 all-gather.1
  46.7 33.6 reduce-scatter.4
  148.8 51.2 reduce-scatter.2
where the time goes:
time: 240 us; the launch traced here: 239 us
  waiting for transfers between devices  103 us (43%)
  starting transfers between devices  71.7 us (30%)
  Pallas kernels  27.2 us (11%)
  between operations  14.2 us (6%)
  local copies, waits for them, and re-layouts  10.9 us (5%)
  matrix products  8.74 us (4%)
  other arithmetic  4.07 us (2%)
    ppermute x14, waiting for transfers between devices, rotate(): lax.ppermute(chunk, axis, [(i, (i + shift) % size) for i in range(size)])  68.3 us
    ppermute x14, starting transfers between devices, rotate(): lax.ppermute(chunk, axis, [(i, (i + shift) % size) for i in range(size)])  51.8 us
    all_gather x1, waiting for transfers between devices, body(): expert_rows = lax.all_gather(normed_experts, 'tp', axis=0, tiled=True)  25.4 us
    ppermute x7, starting transfers between devices, body(): lax.ppermute(key_values, 'ep', [(i, i + k) for i in range(ep_size - k)])  17 us
    pallas_call x2, Pallas kernels, routed_part(): pl.pallas_call(kernel, out_shape=jax.ShapeDtypeStruct(rows.shape, jnp.bfl...  13 us
    unnamed x65, local copies, waits for them, and re-layouts  5.63 us
    ppermute x7, waiting for transfers between devices, body(): lax.ppermute(key_values, 'ep', [(i, i + k) for i in range(ep_size - k)])  5.03 us
  transfers between devices with their start and end apart: 33, of which 17 were waited for; matrix products, arithmetic and copies ran while one was open for 2% of the time, Pallas kernels for 11%

commit v1 on v0

--- a/solution.py
+++ b/solution.py
@@ -323,6 +323,9 @@
     gates = tp_blocks(expert_gate, tp_size)
     ups = tp_blocks(expert_up, tp_size)
     downs = tp_blocks(expert_down, tp_size)
+    shared_weights = [
+        tp_blocks(weight, tp_size) for weight in (shared_gate, shared_up, shared_down)
+    ]
 
     token_rows, model_width = expert_input.shape
     normed_experts = normalize(expert_input, expert_gain)
@@ -342,8 +345,6 @@
     outgoing = jnp.dot(select, normed_experts, preferred_element_type=jnp.float32).astype(
         jnp.bfloat16
     )
-    outgoing, normed_experts = lax.optimization_barrier((outgoing, normed_experts))
-    expert_rows = lax.all_gather(normed_experts, "tp", axis=0, tiled=True)
     span = experts_local * capacity
     received = exchange(
         [outgoing[k * span : (k + 1) * span] for k in range(ep_size)], ep_rank, ep_size, 1
@@ -364,13 +365,7 @@
     )
     mixer_sum = lax.psum_scatter(mixer_part, "tp", scatter_dimension=0, tiled=True)
 
-    shared_gated = jnp.dot(expert_rows, shared_gate, preferred_element_type=jnp.float32)
-    shared_lifted = jnp.dot(expert_rows, shared_up, preferred_element_type=jnp.float32)
-    shared_hidden = (jax.nn.silu(shared_gated) * shared_lifted).astype(jnp.bfloat16)
-    shared_part = jnp.dot(shared_hidden, shared_down, preferred_element_type=jnp.float32)
-    shared_sum = lax.psum_scatter(
-        shared_part.astype(jnp.bfloat16), "tp", scatter_dimension=0, tiled=True
-    )
+    shared_sum = routed_part(normed_experts, *shared_weights, None, False)
 
     slot_rows = stack(received).reshape(ep_size, experts_local, capacity, model_width)
     half = max(1, tp_size // 2)

time: 240 us -> 232 us (0.967)
  waiting for transfers between devices: 103 us -> 80.8 us
  starting transfers between devices: 71.7 us -> 88.1 us
  matrix products: 8.74 us -> 0.49 us
  Pallas kernels: 27.2 us -> 32.4 us
  local copies, waits for them, and re-layouts: 10.9 us -> 13.9 us
  other arithmetic: 4.07 us -> 1.21 us
    ppermute x9 -> x18, waiting for transfers between devices: 3.77 us -> 61 us  [tp_blocks(): blocks = blocks + [lax.ppermute(block, 'tp', pairs) for block in blocks]]
    ppermute x14, waiting for transfers between devices: 68.3 us -> 19.8 us  [rotate(): lax.ppermute(chunk, axis, [(i, (i + shift) % size) for i in range(size)])]
    all_gather x1 -> x0, waiting for transfers between devices: 25.4 us -> none  [body(): expert_rows = lax.all_gather(normed_experts, 'tp', axis=0, tiled=True)]
    ppermute x9 -> x18, starting transfers between devices: 2.73 us -> 11.4 us  [tp_blocks(): blocks = blocks + [lax.ppermute(block, 'tp', pairs) for block in blocks]]
    dot_general x2 -> x0, matrix products: 7.15 us -> none  [the longest x1 4.71 us: body(): jnp.dot(shared_hidden, shared_down, preferred_element_type=jnp.float32)]
    pallas_call x2 -> x3, Pallas kernels: 13 us -> 18.1 us  [routed_part(): pl.pallas_call(kernel, out_shape=jax.ShapeDtypeStruct(rows.shape, jnp.bfl...]
    ppermute x7, waiting for transfers between devices: 5.03 us -> 0.02 us  [body(): lax.ppermute(key_values, 'ep', [(i, i + k) for i in range(ep_size - k)])]
    ppermute x14, starting transfers between devices: 51.8 us -> 56.6 us  [rotate(): lax.ppermute(chunk, axis, [(i, (i + shift) % size) for i in range(size)])]
  transfers between devices with their start and end apart: 33 -> 40, of which waited for: 17 -> 8; matrix products, arithmetic and copies ran while one was open for 2% -> 3% of each run, Pallas kernels for 11% -> 12%
where the time goes in v1:
time: 232 us; the launch traced here: 231 us
  starting transfers between devices  88.1 us (38%)
  waiting for transfers between devices  80.8 us (35%)
  Pallas kernels  32.4 us (14%)
  between operations  14.5 us (6%)
  local copies, waits for them, and re-layouts  13.9 us (6%)
    ppermute x18, waiting for transfers between devices, tp_blocks(): blocks = blocks + [lax.ppermute(block, 'tp', pairs) for block in blocks]  61 us
    ppermute x14, starting transfers between devices, rotate(): lax.ppermute(chunk, axis, [(i, (i + shift) % size) for i in range(size)])  56.6 us
    ppermute x7, starting transfers between devices, body(): lax.ppermute(key_values, 'ep', [(i, i + k) for i in range(ep_size - k)])  20.1 us
    ppermute x14, waiting for transfers between devices, rotate(): lax.ppermute(chunk, axis, [(i, (i + shift) % size) for i in range(size)])  19.8 us
    pallas_call x3, Pallas kernels, routed_part(): pl.pallas_call(kernel, out_shape=jax.ShapeDtypeStruct(rows.shape, jnp.bfl...  18.1 us
    ppermute x18, starting transfers between devices, tp_blocks(): blocks = blocks + [lax.ppermute(block, 'tp', pairs) for block in blocks]  11.4 us
    unnamed x79, local copies, waits for them, and re-layouts  9.63 us
  transfers between devices with their start and end apart: 40, of which 8 were waited for; matrix products, arithmetic and copies ran while one was open for 3% of the time, Pallas kernels for 12%

profile of v1, /device:TPU:0, one launch (start us, length us, event | category | flops | bytes accessed | tf_op | source)
XLA Modules:
  0.0 231.3 jit_solution(275024034812184548)
XLA Ops:
  7.2 4.3 %project.1 = (bf16[256,256]{1,0:T(8,128)(2,1)}, bf16[256,256]{1,0:T(8,128)(2,1)}) custom-call(bf16[256,2048]{1,0:T(8,128)(2,1)} %rows_ref.1, f32[1,2048]{1,0:T(1,128)} %bitcast.35, bf16[2048,128]{1,0:T(8,128)(2,1)} %one.1, bf16[2048,128]{1,0:T(8,128)(2,1)} %two.1, bf16[64,2048]{1,0:T(8,128)(2,1)} %bitcast.33, bf16[64,2048]{1,0:T(8,128)(2,1)} %bitcast.34, ...), custom_call_target="tpu_custom_call" | custom-call | flops 2000000000 | bytes 4000000 | tf_op jit(solution)/shard_map/project/pallas_call | solution.py:63
  11.6 5.0 %collective-permute-start = (bf16[256,256]{1,0:T(8,128)(2,1)}, bf16[256,256]{1,0:T(8,128)(2,1)S(1)}, u32[]{:S(2)}, u32[]{:S(2)}) collective-permute-start(bf16[256,256]{1,0:T(8,128)(2,1)} %get-tuple-element.5.refs_3_), channel_id=1, source_target_pairs={{0,4},{4,8},{8,12},{12,16},{16,20},{20,24},{24,28},{1,5},{5,9},{9,... | collective-permute-start | bytes 393224 | tf_op jit(solution)/shard_map/ppermute | solution.py:358
  16.6 3.5 %collective-permute-start.1 = (bf16[256,256]{1,0:T(8,128)(2,1)}, bf16[256,256]{1,0:T(8,128)(2,1)S(1)}, u32[]{:S(2)}, u32[]{:S(2)}) collective-permute-start(bf16[256,256]{1,0:T(8,128)(2,1)} %get-tuple-element.5.refs_3_), channel_id=1, source_target_pairs={{0,8},{4,12},{8,16},{12,20},{16,24},{20,28},{1,9},{5,13},{9,17},{1... | collective-permute-start | bytes 393224 | tf_op jit(solution)/shard_map/ppermute | solution.py:358
  20.1 5.1 %collective-permute-start.2 = (bf16[256,256]{1,0:T(8,128)(2,1)}, bf16[256,256]{1,0:T(8,128)(2,1)}, u32[]{:S(2)}, u32[]{:S(2)}) collective-permute-start(bf16[256,256]{1,0:T(8,128)(2,1)} %get-tuple-element.5.refs_3_), channel_id=1, source_target_pairs={{0,12},{4,16},{8,20},{12,24},{16,28},{1,13},{5,17},{9,21},{13,25},... | collective-permute-start | bytes 393224 | tf_op jit(solution)/shard_map/ppermute | solution.py:358
  25.2 1.9 collective-permute-start.3
  27.1 1.9 collective-permute-start.4
  29.2 0.1 copy.48
  29.5 0.1 eq.40
  29.6 0.6 reduce-window.6
  30.2 0.2 slice_reduce_fusion
  30.6 0.1 reduce_sum.21
  30.9 0.2 fusion
  31.1 0.2 fusion.2.refs_0_
  31.3 0.5 convolution_convert_fusion
  31.9 0.1 copy-done.34
  32.0 1.3 collective-permute-start.5
  33.3 1.3 collective-permute-start.6
  34.8 1.6 collective-permute-start.25
  36.3 0.8 fusion.9
  37.2 0.9 collective-permute-start.16
  38.1 7.1 %collective-permute-start.17 = (bf16[40,2048]{1,0:T(8,128)(2,1)S(1)}, bf16[40,2048]{1,0:T(8,128)(2,1)S(1)}, u32[]{:S(2)}, u32[]{:S(2)}) collective-permute-start(bf16[40,2048]{1,0:T(8,128)(2,1)S(1)} %get-tuple-element.21), channel_id=1, source_target_pairs={{0,8},{4,12},{8,16},{12,20},{16,24},{20,28},{24,0},{28,4},{1,9},{5... | collective-permute-start | bytes 491528 | tf_op jit(solution)/shard_map/ppermute | solution.py:22
  45.2 4.3 %collective-permute-start.18 = (bf16[40,2048]{1,0:T(8,128)(2,1)S(1)}, bf16[40,2048]{1,0:T(8,128)(2,1)S(1)}, u32[]{:S(2)}, u32[]{:S(2)}) collective-permute-start(bf16[40,2048]{1,0:T(8,128)(2,1)S(1)} %get-tuple-element.20), channel_id=1, source_target_pairs={{0,12},{4,16},{8,20},{12,24},{16,28},{20,0},{24,4},{28,8},{1,13},{... | collective-permute-start | bytes 491528 | tf_op jit(solution)/shard_map/ppermute | solution.py:22
  49.6 3.5 %collective-permute-done.16.refs_1_ = bf16[40,2048]{1,0:T(8,128)(2,1)S(1)} collective-permute-done((bf16[40,2048]{1,0:T(8,128)(2,1)S(1)}, bf16[40,2048]{1,0:T(8,128)(2,1)S(1)}, u32[]{:S(2)}, u32[]{:S(2)}) %collective-permute-start.16) | collective-permute-done | bytes 163872 | tf_op jit(solution)/shard_map/ppermute | solution.py:22
  53.0 0.5 collective-permute-done.17.refs_2_
  53.5 16.5 %collective-permute-start.20 = (bf16[40,2048]{1,0:T(8,128)(2,1)S(1)}, bf16[40,2048]{1,0:T(8,128)(2,1)S(1)}, u32[]{:S(2)}, u32[]{:S(2)}) collective-permute-start(bf16[40,2048]{1,0:T(8,128)(2,1)S(1)} %get-tuple-element.18), channel_id=1, source_target_pairs={{0,20},{4,24},{8,28},{12,0},{16,4},{20,8},{24,12},{28,16},{1,21},{... | collective-permute-start | bytes 491528 | tf_op jit(solution)/shard_map/ppermute | solution.py:22
  70.1 3.5 %collective-permute-start.21 = (bf16[40,2048]{1,0:T(8,128)(2,1)S(1)}, bf16[40,2048]{1,0:T(8,128)(2,1)S(1)}, u32[]{:S(2)}, u32[]{:S(2)}) collective-permute-start(bf16[40,2048]{1,0:T(8,128)(2,1)S(1)} %get-tuple-element.17), channel_id=1, source_target_pairs={{0,24},{4,28},{8,0},{12,4},{16,8},{20,12},{24,16},{28,20},{1,25},{... | collective-permute-start | bytes 491528 | tf_op jit(solution)/shard_map/ppermute | solution.py:22
  73.6 1.7 collective-permute-start.22
  75.3 1.4 collective-permute-start.27
  76.7 2.1 collective-permute-start.23
  78.8 0.2 collective-permute-done.22.refs_7_
  79.0 1.6 collective-permute-start.10
  80.6 51.6 %collective-permute-done.10.refs_6_ = bf16[2048,128]{1,0:T(8,128)(2,1)S(1)} collective-permute-done((bf16[2048,128]{1,0:T(8,128)(2,1)S(1)}, bf16[2048,128]{1,0:T(8,128)(2,1)S(1)}, u32[]{:S(2)}, u32[]{:S(2)}) %collective-permute-start.10) | collective-permute-done | bytes 524320 | tf_op jit(solution)/shard_map/ppermute | solution.py:136
  132.2 1.0 copy-done.2
  133.2 0.5 collective-permute-start.31
  133.7 0.5 collective-permute-start.28
  134.3 4.3 %attention.1 = bf16[256,2048]{1,0:T(8,128)(2,1)} custom-call(s32[1]{0:T(128)} %bitcast.refs_0_, f32[2]{0:T(128)} %refs_1_.2, bf16[256,256]{1,0:T(8,128)(2,1)} %get-tuple-element.4.refs_2_, bf16[256,256]{1,0:T(8,128)(2,1)} %get-tuple-element.5.refs_3_, f32[1,128]{1,0:T(1,128)} %bitcast.36, bf16[256,2048]{1,0:T(8,128)(2,1)} %refs_5_.2, ...), custom_call_target="tpu_custom_call" | custom-call | flops 6000000000 | bytes 4000000 | tf_op jit(solution)/shard_map/attention/pallas_call | solution.py:243
  138.7 2.6 %stack.1 = bf16[8,40,2048]{2,1,0:T(8,128)(2,1)} custom-call(bf16[40,2048]{1,0:T(8,128)(2,1)} %get-tuple-element.23.refs_0_, bf16[40,2048]{1,0:T(8,128)(2,1)} %copy-done.18, bf16[40,2048]{1,0:T(8,128)(2,1)} %copy-done.19, bf16[40,2048]{1,0:T(8,128)(2,1)} %copy-done.20, bf16[40,2048]{1,0:T(8,128)(2,1)} %copy-done.21, bf16[40,2048]{1,0:T(8,128)(2,1)} %copy-done.22, ...), custom_call_target="tpu_custom_call" | custom-call | tf_op jit(solution)/shard_map/stack/pallas_call | solution.py:87
  141.3 0.4 collective-permute-start.11
  141.7 1.7 collective-permute-start.13
  143.5 0.3 collective-permute-start.7
  143.8 1.2 copy-done.3
  145.0 6.0 %routed.4.refs_7_ = f32[320,2048]{1,0:T(8,128)} custom-call(bf16[320,2048]{1,0:T(8,128)(2,1)} %bitcast.31, bf16[2048,256]{1,0:T(8,128)(2,1)S(1)} %bitcast.28, bf16[2048,256]{1,0:T(8,128)(2,1)S(1)} %bitcast.30, bf16[2048,256]{1,0:T(8,128)(2,1)S(1)} %bitcast.29, bf16[2048,256]{1,0:T(8,128)(2,1)} %bitcast.17.refs_4_, bf16[256,2048]{1,0:T(8,128)(2,1)} %bitcast.18.refs_5_, ...), custom_call_target="tpu_custom_call" | custom-call | flops 4000000000 | bytes 8000000 | tf_op jit(solution)/shard_map/routed/pallas_call | solution.py:118
  151.0 0.5 collective-permute-start.8
  151.5 7.6 %routed.5 = bf16[320,2048]{1,0:T(8,128)(2,1)} custom-call(bf16[320,2048]{1,0:T(8,128)(2,1)} %bitcast.32, bf16[2048,256]{1,0:T(8,128)(2,1)} %bitcast.8.refs_1_, bf16[2048,256]{1,0:T(8,128)(2,1)} %bitcast.9.refs_2_, bf16[2048,256]{1,0:T(8,128)(2,1)} %bitcast.10.refs_3_, bf16[2048,256]{1,0:T(8,128)(2,1)} %bitcast.11.refs_4_, ...), custom_call_target="tpu_custom_call" | custom-call | flops 4000000000 | bytes 8000000 | tf_op jit(solution)/shard_map/routed/pallas_call | solution.py:118
  159.1 0.1 collective-permute-start.12
  159.2 9.3 %collective-permute-done.7.refs_2_ = bf16[2048,128]{1,0:T(8,128)(2,1)} collective-permute-done((bf16[2048,128]{1,0:T(8,128)(2,1)S(1)}, bf16[2048,128]{1,0:T(8,128)(2,1)}, u32[]{:S(2)}, u32[]{:S(2)}) %collective-permute-start.7) | collective-permute-done | bytes 524320 | tf_op jit(solution)/shard_map/ppermute | solution.py:136
  168.6 0.5 collective-permute-start.9
  169.1 2.5 %fusion.8 = (bf16[40,2048]{1,0:T(8,128)(2,1)S(1)}, bf16[40,2048]{1,0:T(8,128)(2,1)}, bf16[40,2048]{1,0:T(8,128)(2,1)}, bf16[40,2048]{1,0:T(8,128)(2,1)}, bf16[40...) fusion(bf16[320,2048]{1,0:T(8,128)(2,1)} %routed.5), kind=kLoop, calls=%fused_computation.23 | loop fusion | bytes 2621440 | tf_op jit(solution)/shard_map/slice | solution.py:389
  171.6 17.4 %collective-permute-start.32 = (bf16[40,2048]{1,0:T(8,128)(2,1)}, bf16[40,2048]{1,0:T(8,128)(2,1)S(1)}, u32[]{:S(2)}, u32[]{:S(2)}) collective-permute-start(bf16[40,2048]{1,0:T(8,128)(2,1)} %get-tuple-element.14), channel_id=1, source_target_pairs={{0,28},{4,0},{8,4},{12,8},{16,12},{20,16},{24,20},{28,24},{1,29},{... | collective-permute-start | bytes 491528 | tf_op jit(solution)/shard_map/ppermute | solution.py:22
  189.0 0.7 copy.50.weight_ref
  189.8 0.8 copy-done.14
  190.6 3.6 %collective-permute-start.35 = (bf16[40,2048]{1,0:T(8,128)(2,1)}, bf16[40,2048]{1,0:T(8,128)(2,1)S(1)}, u32[]{:S(2)}, u32[]{:S(2)}) collective-permute-start(bf16[40,2048]{1,0:T(8,128)(2,1)} %get-tuple-element.11), channel_id=1, source_target_pairs={{0,16},{4,20},{8,24},{12,28},{16,0},{20,4},{24,8},{28,12},{1,17},{... | collective-permute-start | bytes 491528 | tf_op jit(solution)/shard_map/ppermute | solution.py:22
  194.2 1.4 collective-permute-start.37
  195.6 1.9 collective-permute-done.33.rest_2_
  197.5 1.0 copy-done.8
  198.5 1.0 copy-done.11
  199.6 1.0 copy-done.13
  200.6 1.0 copy-done.15
  201.7 4.5 %routed.3.shared_ref = f32[128,2048]{1,0:T(8,128)} custom-call(bf16[128,2048]{1,0:T(8,128)(2,1)S(1)} %fusion.2.refs_0_, bf16[2048,128]{1,0:T(8,128)(2,1)S(1)} %copy-done.4, bf16[2048,128]{1,0:T(8,128)(2,1)} %collective-permute-done.7.refs_2_, bf16[2048,128]{1,0:T(8,128)(2,1)S(1)} %collective-permute-done.8.refs_3_, ...), custom_call_target="tpu_custom_call" | custom-call | flops 8000000000 | bytes 8000000 | tf_op jit(solution)/shard_map/routed/pallas_call | solution.py:118
  206.2 7.8 %collective-permute-done.35.rest_4_ = bf16[40,2048]{1,0:T(8,128)(2,1)S(1)} collective-permute-done((bf16[40,2048]{1,0:T(8,128)(2,1)}, bf16[40,2048]{1,0:T(8,128)(2,1)S(1)}, u32[]{:S(2)}, u32[]{:S(2)}) %collective-permute-start.35) | collective-permute-done | bytes 163872 | tf_op jit(solution)/shard_map/ppermute | solution.py:22
  214.0 5.9 %collective-permute-done.36.rest_5_ = bf16[40,2048]{1,0:T(8,128)(2,1)S(1)} collective-permute-done((bf16[40,2048]{1,0:T(8,128)(2,1)}, bf16[40,2048]{1,0:T(8,128)(2,1)S(1)}, u32[]{:S(2)}, u32[]{:S(2)}) %collective-permute-start.36) | collective-permute-done | bytes 163872 | tf_op jit(solution)/shard_map/ppermute | solution.py:22
  220.0 0.6 copy-done.27
  220.7 0.7 copy-done.29
  221.3 3.1 %combine.1 = bf16[128,2048]{1,0:T(8,128)(2,1)} custom-call(s32[128,2]{1,0:T(8,128)} %copy-done.17, f32[128,2]{1,0:T(8,128)} %copy.50.weight_ref, f32[128,2048]{1,0:T(8,128)} %routed.3.shared_ref, bf16[40,2048]{1,0:T(8,128)(2,1)} %get-tuple-element.15.rest_0_, bf16[40,2048]{1,0:T(8,128)(2,1)} %copy-done.24, bf16[40,2048]{1,0:T(8,128)(2,1)} %collective-permute-done.33.rest_2_, ...), custom_call_target="tpu_custom_call" | custom-call | tf_op jit(solution)/shard_map/combine/pallas_call | solution.py:277
  (125 shorter events, 1.1 us)
Async XLA Ops:
  7.2 217.3 %reduce-scatter.2.cloned.1.call-start = ((), (), s32[]{:S(2)}) async-start(), calls=%async_computation.1 | async-start | bytes 1310720 | tf_op jit(solution)/shard_map/reduce_scatter | solution.py:366
  7.2 21.8 %copy-start.32 = (s32[128,2]{0,1:T(2,128)S(1)}, s32[128,2]{0,1:T(2,128)}, u32[]{:S(2)}) copy-start(s32[128,2]{0,1:T(2,128)} %param.32) | copy-start | bytes 3076
  7.2 23.7 %copy-start.16 = (bf16[128,2048]{1,0:T(8,128)(2,1)S(1)}, bf16[128,2048]{1,0:T(8,128)(2,1)}, u32[]{:S(2)}) copy-start(bf16[128,2048]{1,0:T(8,128)(2,1)} %param.30) | copy-start | bytes 1572868
  11.6 19.5 %copy-start.30 = (f32[2048]{0:T(1024)S(1)}, f32[2048]{0:T(1024)}, u32[]{:S(2)}) copy-start(f32[2048]{0:T(1024)} %param.31) | copy-start | bytes 24580
  11.6 20.3 %collective-permute-start = (bf16[256,256]{1,0:T(8,128)(2,1)}, bf16[256,256]{1,0:T(8,128)(2,1)S(1)}, u32[]{:S(2)}, u32[]{:S(2)}) collective-permute-start(bf16[256,256]{1,0:T(8,128)(2,1)} %get-tuple-element.5.refs_3_), channel_id=1, source_target_pairs={{0,4},{4,8},{8,12},{12,16},{16,20},{20,24},{24,28},{1,5},{5,9},{9,... | collective-permute-start | bytes 393224 | tf_op jit(solution)/shard_map/ppermute | solution.py:358
  16.6 16.8 %collective-permute-start.1 = (bf16[256,256]{1,0:T(8,128)(2,1)}, bf16[256,256]{1,0:T(8,128)(2,1)S(1)}, u32[]{:S(2)}, u32[]{:S(2)}) collective-permute-start(bf16[256,256]{1,0:T(8,128)(2,1)} %get-tuple-element.5.refs_3_), channel_id=1, source_target_pairs={{0,8},{4,12},{8,16},{12,20},{16,24},{20,28},{1,9},{5,13},{9,17},{1... | collective-permute-start | bytes 393224 | tf_op jit(solution)/shard_map/ppermute | solution.py:358
  20.1 14.6 %collective-permute-start.2 = (bf16[256,256]{1,0:T(8,128)(2,1)}, bf16[256,256]{1,0:T(8,128)(2,1)}, u32[]{:S(2)}, u32[]{:S(2)}) collective-permute-start(bf16[256,256]{1,0:T(8,128)(2,1)} %get-tuple-element.5.refs_3_), channel_id=1, source_target_pairs={{0,12},{4,16},{8,20},{12,24},{16,28},{1,13},{5,17},{9,21},{13,25},... | collective-permute-start | bytes 393224 | tf_op jit(solution)/shard_map/ppermute | solution.py:358
  25.2 9.5 %collective-permute-start.3 = (bf16[256,256]{1,0:T(8,128)(2,1)}, bf16[256,256]{1,0:T(8,128)(2,1)}, u32[]{:S(2)}, u32[]{:S(2)}) collective-permute-start(bf16[256,256]{1,0:T(8,128)(2,1)} %get-tuple-element.5.refs_3_), channel_id=1, source_target_pairs={{0,16},{4,20},{8,24},{12,28},{1,17},{5,21},{9,25},{13,29},{2,18},{... | collective-permute-start | bytes 393224 | tf_op jit(solution)/shard_map/ppermute | solution.py:358
  27.1 10.0 %collective-permute-start.4 = (bf16[256,256]{1,0:T(8,128)(2,1)}, bf16[256,256]{1,0:T(8,128)(2,1)}, u32[]{:S(2)}, u32[]{:S(2)}) collective-permute-start(bf16[256,256]{1,0:T(8,128)(2,1)} %get-tuple-element.5.refs_3_), channel_id=1, source_target_pairs={{0,20},{4,24},{8,28},{1,21},{5,25},{9,29},{2,22},{6,26},{10,30},{3... | collective-permute-start | bytes 393224 | tf_op jit(solution)/shard_map/ppermute | solution.py:358
  31.1 3.5 %copy-start = (bf16[1,2048,256]{2,1,0:T(8,128)(2,1)S(1)}, bf16[1,2048,256]{2,1,0:T(8,128)(2,1)}, u32[]{:S(2)}) copy-start(bf16[1,2048,256]{2,1,0:T(8,128)(2,1)} %param.34) | copy-start | bytes 3145732
  31.1 3.6 %copy-start.1 = (bf16[1,2048,256]{2,1,0:T(8,128)(2,1)S(1)}, bf16[1,2048,256]{2,1,0:T(8,128)(2,1)}, u32[]{:S(2)}) copy-start(bf16[1,2048,256]{2,1,0:T(8,128)(2,1)} %param.35) | copy-start | bytes 3145732
  31.8 47.1 %copy-start.5 = (bf16[2048,128]{1,0:T(8,128)(2,1)S(1)}, bf16[2048,128]{1,0:T(8,128)(2,1)}, u32[]{:S(2)}) copy-start(bf16[2048,128]{1,0:T(8,128)(2,1)} %refs_5_.3) | copy-start | bytes 1572868
  32.0 5.2 %copy-start.35 = (bf16[256,256]{1,0:T(8,128)(2,1)}, bf16[256,256]{1,0:T(8,128)(2,1)S(1)}, u32[]{:S(2)}) copy-start(bf16[256,256]{1,0:T(8,128)(2,1)S(1)} %collective-permute-done.refs_6_) | copy-start | bytes 393220
  32.0 6.1 %collective-permute-start.5 = (bf16[256,256]{1,0:T(8,128)(2,1)S(1)}, bf16[256,256]{1,0:T(8,128)(2,1)S(1)}, u32[]{:S(2)}, u32[]{:S(2)}) collective-permute-start(bf16[256,256]{1,0:T(8,128)(2,1)S(1)} %copy-done.34), channel_id=1, source_target_pairs={{0,24},{4,28},{1,25},{5,29},{2,26},{6,30},{3,27},{7,31}} | collective-permute-start | bytes 393224 | tf_op jit(solution)/shard_map/ppermute | solution.py:358
  33.3 3.9 %copy-start.36 = (bf16[256,256]{1,0:T(8,128)(2,1)}, bf16[256,256]{1,0:T(8,128)(2,1)S(1)}, u32[]{:S(2)}) copy-start(bf16[256,256]{1,0:T(8,128)(2,1)S(1)} %collective-permute-done.1.refs_7_) | copy-start | bytes 393220
  33.3 11.9 %collective-permute-start.6 = (bf16[256,256]{1,0:T(8,128)(2,1)S(1)}, bf16[256,256]{1,0:T(8,128)(2,1)S(1)}, u32[]{:S(2)}, u32[]{:S(2)}) collective-permute-start(bf16[256,256]{1,0:T(8,128)(2,1)S(1)} %copy-done.34), channel_id=1, source_target_pairs={{0,28},{1,29},{2,30},{3,31}} | collective-permute-start | bytes 393224 | tf_op jit(solution)/shard_map/ppermute | solution.py:358
  34.7 97.5 %collective-permute-start.29 = (bf16[1,2048,256]{2,1,0:T(8,128)(2,1)S(1)}, bf16[1,2048,256]{2,1,0:T(8,128)(2,1)S(1)}, u32[]{:S(2)}, u32[]{:S(2)}) collective-permute-start(bf16[1,2048,256]{2,1,0:T(8,128)(2,1)S(1)} %copy-done), channel_id=1, source_target_pairs={{0,1},{1,0},{2,3},{3,2},{4,5},{5,4},{6,7},{7,6},{8,9},{9,8},{10,11... | collective-permute-start | bytes 3145736 | tf_op jit(solution)/shard_map/ppermute | solution.py:136
  34.8 99.0 %collective-permute-start.25 = (bf16[1,2048,256]{2,1,0:T(8,128)(2,1)S(1)}, bf16[1,2048,256]{2,1,0:T(8,128)(2,1)}, u32[]{:S(2)}, u32[]{:S(2)}) collective-permute-start(bf16[1,2048,256]{2,1,0:T(8,128)(2,1)S(1)} %copy-done.1), channel_id=1, source_target_pairs={{0,2},{1,3},{2,0},{3,1},{4,6},{5,7},{6,4},{7,5},{8,10},{9,11},{10,... | collective-permute-start | bytes 3145736 | tf_op jit(solution)/shard_map/ppermute | solution.py:136
  37.2 15.9 %collective-permute-start.16 = (bf16[40,2048]{1,0:T(8,128)(2,1)S(1)}, bf16[40,2048]{1,0:T(8,128)(2,1)S(1)}, u32[]{:S(2)}, u32[]{:S(2)}) collective-permute-start(bf16[40,2048]{1,0:T(8,128)(2,1)S(1)} %get-tuple-element.22), channel_id=1, source_target_pairs={{0,4},{4,8},{8,12},{12,16},{16,20},{20,24},{24,28},{28,0},{1,5},{5... | collective-permute-start | bytes 491528 | tf_op jit(solution)/shard_map/ppermute | solution.py:22
  38.1 7.2 %copy-start.37 = (bf16[256,256]{1,0:T(8,128)(2,1)}, bf16[256,256]{1,0:T(8,128)(2,1)S(1)}, u32[]{:S(2)}) copy-start(bf16[256,256]{1,0:T(8,128)(2,1)S(1)} %collective-permute-done.5.refs_11_) | copy-start | bytes 393220
  38.1 15.4 %collective-permute-start.17 = (bf16[40,2048]{1,0:T(8,128)(2,1)S(1)}, bf16[40,2048]{1,0:T(8,128)(2,1)S(1)}, u32[]{:S(2)}, u32[]{:S(2)}) collective-permute-start(bf16[40,2048]{1,0:T(8,128)(2,1)S(1)} %get-tuple-element.21), channel_id=1, source_target_pairs={{0,8},{4,12},{8,16},{12,20},{16,24},{20,28},{24,0},{28,4},{1,9},{5... | collective-permute-start | bytes 491528 | tf_op jit(solution)/shard_map/ppermute | solution.py:22
  45.2 89.1 %copy-start.38 = (bf16[256,256]{1,0:T(8,128)(2,1)}, bf16[256,256]{1,0:T(8,128)(2,1)S(1)}, u32[]{:S(2)}) copy-start(bf16[256,256]{1,0:T(8,128)(2,1)S(1)} %collective-permute-done.6.refs_12_) | copy-start | bytes 393220
  45.2 24.8 %collective-permute-start.18 = (bf16[40,2048]{1,0:T(8,128)(2,1)S(1)}, bf16[40,2048]{1,0:T(8,128)(2,1)S(1)}, u32[]{:S(2)}, u32[]{:S(2)}) collective-permute-start(bf16[40,2048]{1,0:T(8,128)(2,1)S(1)} %get-tuple-element.20), channel_id=1, source_target_pairs={{0,12},{4,16},{8,20},{12,24},{16,28},{20,0},{24,4},{28,8},{1,13},{... | collective-permute-start | bytes 491528 | tf_op jit(solution)/shard_map/ppermute | solution.py:22
  53.0 85.6 %copy-start.18 = (bf16[40,2048]{1,0:T(8,128)(2,1)}, bf16[40,2048]{1,0:T(8,128)(2,1)S(1)}, u32[]{:S(2)}) copy-start(bf16[40,2048]{1,0:T(8,128)(2,1)S(1)} %collective-permute-done.16.refs_1_) | copy-start | bytes 491524
  53.0 20.5 %collective-permute-start.19 = (bf16[40,2048]{1,0:T(8,128)(2,1)S(1)}, bf16[40,2048]{1,0:T(8,128)(2,1)S(1)}, u32[]{:S(2)}, u32[]{:S(2)}) collective-permute-start(bf16[40,2048]{1,0:T(8,128)(2,1)S(1)} %get-tuple-element.19), channel_id=1, source_target_pairs={{0,16},{4,20},{8,24},{12,28},{16,0},{20,4},{24,8},{28,12},{1,17},{... | collective-permute-start | bytes 491528 | tf_op jit(solution)/shard_map/ppermute | solution.py:22
  53.5 85.1 %copy-start.19 = (bf16[40,2048]{1,0:T(8,128)(2,1)}, bf16[40,2048]{1,0:T(8,128)(2,1)S(1)}, u32[]{:S(2)}) copy-start(bf16[40,2048]{1,0:T(8,128)(2,1)S(1)} %collective-permute-done.17.refs_2_) | copy-start | bytes 491524
  53.5 21.8 %collective-permute-start.20 = (bf16[40,2048]{1,0:T(8,128)(2,1)S(1)}, bf16[40,2048]{1,0:T(8,128)(2,1)S(1)}, u32[]{:S(2)}, u32[]{:S(2)}) collective-permute-start(bf16[40,2048]{1,0:T(8,128)(2,1)S(1)} %get-tuple-element.18), channel_id=1, source_target_pairs={{0,20},{4,24},{8,28},{12,0},{16,4},{20,8},{24,12},{28,16},{1,21},{... | collective-permute-start | bytes 491528 | tf_op jit(solution)/shard_map/ppermute | solution.py:22
  70.1 68.6 %copy-start.20 = (bf16[40,2048]{1,0:T(8,128)(2,1)}, bf16[40,2048]{1,0:T(8,128)(2,1)S(1)}, u32[]{:S(2)}) copy-start(bf16[40,2048]{1,0:T(8,128)(2,1)S(1)} %collective-permute-done.18.refs_3_) | copy-start | bytes 491524
  70.1 6.7 %collective-permute-start.21 = (bf16[40,2048]{1,0:T(8,128)(2,1)S(1)}, bf16[40,2048]{1,0:T(8,128)(2,1)S(1)}, u32[]{:S(2)}, u32[]{:S(2)}) collective-permute-start(bf16[40,2048]{1,0:T(8,128)(2,1)S(1)} %get-tuple-element.17), channel_id=1, source_target_pairs={{0,24},{4,28},{8,0},{12,4},{16,8},{20,12},{24,16},{28,20},{1,25},{... | collective-permute-start | bytes 491528 | tf_op jit(solution)/shard_map/ppermute | solution.py:22
  73.6 65.1 %copy-start.21 = (bf16[40,2048]{1,0:T(8,128)(2,1)}, bf16[40,2048]{1,0:T(8,128)(2,1)S(1)}, u32[]{:S(2)}) copy-start(bf16[40,2048]{1,0:T(8,128)(2,1)S(1)} %collective-permute-done.19.refs_4_) | copy-start | bytes 491524
  73.6 5.4 %collective-permute-start.22 = (bf16[40,2048]{1,0:T(8,128)(2,1)S(1)}, bf16[40,2048]{1,0:T(8,128)(2,1)}, u32[]{:S(2)}, u32[]{:S(2)}) collective-permute-start(bf16[40,2048]{1,0:T(8,128)(2,1)S(1)} %get-tuple-element.16), channel_id=1, source_target_pairs={{0,28},{4,0},{8,4},{12,8},{16,12},{20,16},{24,20},{28,24},{1,29},{... | collective-permute-start | bytes 491528 | tf_op jit(solution)/shard_map/ppermute | solution.py:22
  75.3 63.3 %copy-start.22 = (bf16[40,2048]{1,0:T(8,128)(2,1)}, bf16[40,2048]{1,0:T(8,128)(2,1)S(1)}, u32[]{:S(2)}) copy-start(bf16[40,2048]{1,0:T(8,128)(2,1)S(1)} %collective-permute-done.20.refs_5_) | copy-start | bytes 491524
  75.3 58.4 %collective-permute-start.27 = (bf16[1,256,2048]{2,1,0:T(8,128)(2,1)}, bf16[1,256,2048]{2,1,0:T(8,128)(2,1)}, u32[]{:S(2)}, u32[]{:S(2)}) collective-permute-start(bf16[1,256,2048]{2,1,0:T(8,128)(2,1)} %param.36), channel_id=1, source_target_pairs={{0,2},{1,3},{2,0},{3,1},{4,6},{5,7},{6,4},{7,5},{8,10},{9,11},{10,... | collective-permute-start | bytes 3145736 | tf_op jit(solution)/shard_map/ppermute | solution.py:136
  76.7 57.5 %collective-permute-start.23 = (bf16[1,2048,256]{2,1,0:T(8,128)(2,1)S(1)}, bf16[1,2048,256]{2,1,0:T(8,128)(2,1)}, u32[]{:S(2)}, u32[]{:S(2)}) collective-permute-start(bf16[1,2048,256]{2,1,0:T(8,128)(2,1)S(1)} %copy-done), channel_id=1, source_target_pairs={{0,2},{1,3},{2,0},{3,1},{4,6},{5,7},{6,4},{7,5},{8,10},{9,11},{10,... | collective-permute-start | bytes 3145736 | tf_op jit(solution)/shard_map/ppermute | solution.py:136
  79.0 53.2 %collective-permute-start.10 = (bf16[2048,128]{1,0:T(8,128)(2,1)S(1)}, bf16[2048,128]{1,0:T(8,128)(2,1)S(1)}, u32[]{:S(2)}, u32[]{:S(2)}) collective-permute-start(bf16[2048,128]{1,0:T(8,128)(2,1)S(1)} %copy-done.5), channel_id=1, source_target_pairs={{0,2},{1,3},{2,0},{3,1},{4,6},{5,7},{6,4},{7,5},{8,10},{9,11},{10,... | collective-permute-start | bytes 1572872 | tf_op jit(solution)/shard_map/ppermute | solution.py:136
  132.2 9.1 %collective-permute-start.30 = (bf16[1,2048,256]{2,1,0:T(8,128)(2,1)S(1)}, bf16[1,2048,256]{2,1,0:T(8,128)(2,1)}, u32[]{:S(2)}, u32[]{:S(2)}) collective-permute-start(bf16[1,2048,256]{2,1,0:T(8,128)(2,1)S(1)} %copy-done.1), channel_id=1, source_target_pairs={{0,1},{1,0},{2,3},{3,2},{4,5},{5,4},{6,7},{7,6},{8,9},{9,8},{10,11... | collective-permute-start | bytes 3145736 | tf_op jit(solution)/shard_map/ppermute | solution.py:136
  133.2 8.5 %collective-permute-start.31 = (bf16[1,256,2048]{2,1,0:T(8,128)(2,1)}, bf16[1,256,2048]{2,1,0:T(8,128)(2,1)}, u32[]{:S(2)}, u32[]{:S(2)}) collective-permute-start(bf16[1,256,2048]{2,1,0:T(8,128)(2,1)} %param.36), channel_id=1, source_target_pairs={{0,1},{1,0},{2,3},{3,2},{4,5},{5,4},{6,7},{7,6},{8,9},{9,8},{10,11... | collective-permute-start | bytes 3145736 | tf_op jit(solution)/shard_map/ppermute | solution.py:136
  133.7 9.8 %collective-permute-start.26 = (bf16[1,2048,256]{2,1,0:T(8,128)(2,1)}, bf16[1,2048,256]{2,1,0:T(8,128)(2,1)}, u32[]{:S(2)}, u32[]{:S(2)}) collective-permute-start(bf16[1,2048,256]{2,1,0:T(8,128)(2,1)} %collective-permute-done.25), channel_id=1, source_target_pairs={{0,1},{1,0},{2,3},{3,2},{4,5},{5,4},{6,7},{7,6},{8,9},{9,8},{10,11... | collective-permute-start | bytes 3145736 | tf_op jit(solution)/shard_map/ppermute | solution.py:136
  133.7 17.2 %collective-permute-start.28 = (bf16[1,256,2048]{2,1,0:T(8,128)(2,1)}, bf16[1,256,2048]{2,1,0:T(8,128)(2,1)}, u32[]{:S(2)}, u32[]{:S(2)}) collective-permute-start(bf16[1,256,2048]{2,1,0:T(8,128)(2,1)} %collective-permute-done.27), channel_id=1, source_target_pairs={{0,1},{1,0},{2,3},{3,2},{4,5},{5,4},{6,7},{7,6},{8,9},{9,8},{10,11... | collective-permute-start | bytes 3145736 | tf_op jit(solution)/shard_map/ppermute | solution.py:136
  134.2 16.8 %collective-permute-start.24 = (bf16[1,2048,256]{2,1,0:T(8,128)(2,1)}, bf16[1,2048,256]{2,1,0:T(8,128)(2,1)}, u32[]{:S(2)}, u32[]{:S(2)}) collective-permute-start(bf16[1,2048,256]{2,1,0:T(8,128)(2,1)} %collective-permute-done.23), channel_id=1, source_target_pairs={{0,1},{1,0},{2,3},{3,2},{4,5},{5,4},{6,7},{7,6},{8,9},{9,8},{10,11... | collective-permute-start | bytes 3145736 | tf_op jit(solution)/shard_map/ppermute | solution.py:136
  138.7 4.8 %copy-start.4 = (bf16[2048,128]{1,0:T(8,128)(2,1)S(1)}, bf16[2048,128]{1,0:T(8,128)(2,1)}, u32[]{:S(2)}) copy-start(bf16[2048,128]{1,0:T(8,128)(2,1)} %refs_1_.3) | copy-start | bytes 1572868
  141.3 27.3 %collective-permute-start.11 = (bf16[2048,128]{1,0:T(8,128)(2,1)}, bf16[2048,128]{1,0:T(8,128)(2,1)S(1)}, u32[]{:S(2)}, u32[]{:S(2)}) collective-permute-start(bf16[2048,128]{1,0:T(8,128)(2,1)} %refs_5_.3), channel_id=1, source_target_pairs={{0,1},{1,0},{2,3},{3,2},{4,5},{5,4},{6,7},{7,6},{8,9},{9,8},{10,11... | collective-permute-start | bytes 1572872 | tf_op jit(solution)/shard_map/ppermute | solution.py:136
  141.7 17.4 %collective-permute-start.13 = (bf16[128,2048]{1,0:T(8,128)(2,1)}, bf16[128,2048]{1,0:T(8,128)(2,1)}, u32[]{:S(2)}, u32[]{:S(2)}) collective-permute-start(bf16[128,2048]{1,0:T(8,128)(2,1)} %refs_9_.1), channel_id=1, source_target_pairs={{0,2},{1,3},{2,0},{3,1},{4,6},{5,7},{6,4},{7,5},{8,10},{9,11},{10,... | collective-permute-start | bytes 1572872 | tf_op jit(solution)/shard_map/ppermute | solution.py:136
  143.5 25.1 %collective-permute-start.7 = (bf16[2048,128]{1,0:T(8,128)(2,1)S(1)}, bf16[2048,128]{1,0:T(8,128)(2,1)}, u32[]{:S(2)}, u32[]{:S(2)}) collective-permute-start(bf16[2048,128]{1,0:T(8,128)(2,1)S(1)} %copy-done.4), channel_id=1, source_target_pairs={{0,2},{1,3},{2,0},{3,1},{4,6},{5,7},{6,4},{7,5},{8,10},{9,11},{10,... | collective-permute-start | bytes 1572872 | tf_op jit(solution)/shard_map/ppermute | solution.py:136
  145.0 6.0 %copy-start.7 = (bf16[128,2048]{1,0:T(8,128)(2,1)S(1)}, bf16[128,2048]{1,0:T(8,128)(2,1)}, u32[]{:S(2)}) copy-start(bf16[128,2048]{1,0:T(8,128)(2,1)} %refs_9_.1) | copy-start | bytes 1572868
  151.0 20.6 %collective-permute-start.14 = (bf16[128,2048]{1,0:T(8,128)(2,1)S(1)}, bf16[128,2048]{1,0:T(8,128)(2,1)S(1)}, u32[]{:S(2)}, u32[]{:S(2)}) collective-permute-start(bf16[128,2048]{1,0:T(8,128)(2,1)S(1)} %copy-done.7), channel_id=1, source_target_pairs={{0,1},{1,0},{2,3},{3,2},{4,5},{5,4},{6,7},{7,6},{8,9},{9,8},{10,11... | collective-permute-start | bytes 1572872 | tf_op jit(solution)/shard_map/ppermute | solution.py:136
  151.0 38.0 %collective-permute-start.8 = (bf16[2048,128]{1,0:T(8,128)(2,1)S(1)}, bf16[2048,128]{1,0:T(8,128)(2,1)S(1)}, u32[]{:S(2)}, u32[]{:S(2)}) collective-permute-start(bf16[2048,128]{1,0:T(8,128)(2,1)S(1)} %copy-done.4), channel_id=1, source_target_pairs={{0,1},{1,0},{2,3},{3,2},{4,5},{5,4},{6,7},{7,6},{8,9},{9,8},{10,11... | collective-permute-start | bytes 1572872 | tf_op jit(solution)/shard_map/ppermute | solution.py:136
  151.5 7.6 %copy-start.10 = (bf16[2048,128]{1,0:T(8,128)(2,1)S(1)}, bf16[2048,128]{1,0:T(8,128)(2,1)}, u32[]{:S(2)}) copy-start(bf16[2048,128]{1,0:T(8,128)(2,1)} %copy-done.9) | copy-start | bytes 1572868
  159.1 29.9 %copy-start.31 = (f32[128,2]{0,1:T(2,128)S(1)}, f32[128,2]{0,1:T(2,128)}, u32[]{:S(2)}) copy-start(f32[128,2]{0,1:T(2,128)} %param.33) | copy-start | bytes 3076
  159.1 38.4 %copy-start.6 = (bf16[2048,128]{1,0:T(8,128)(2,1)S(1)}, bf16[2048,128]{1,0:T(8,128)(2,1)}, u32[]{:S(2)}) copy-start(bf16[2048,128]{1,0:T(8,128)(2,1)} %refs_5_.3) | copy-start | bytes 1572868
  159.1 30.7 %collective-permute-start.12 = (bf16[2048,128]{1,0:T(8,128)(2,1)S(1)}, bf16[2048,128]{1,0:T(8,128)(2,1)S(1)}, u32[]{:S(2)}, u32[]{:S(2)}) collective-permute-start(bf16[2048,128]{1,0:T(8,128)(2,1)S(1)} %copy-done.10), channel_id=1, source_target_pairs={{0,1},{1,0},{2,3},{3,2},{4,5},{5,4},{6,7},{7,6},{8,9},{9,8},{10,11... | collective-permute-start | bytes 1572872 | tf_op jit(solution)/shard_map/ppermute | solution.py:136
  168.6 22.0 %collective-permute-start.15 = (bf16[128,2048]{1,0:T(8,128)(2,1)}, bf16[128,2048]{1,0:T(8,128)(2,1)}, u32[]{:S(2)}, u32[]{:S(2)}) collective-permute-start(bf16[128,2048]{1,0:T(8,128)(2,1)} %collective-permute-done.13.refs_10_), channel_id=1, source_target_pairs={{0,1},{1,0},{2,3},{3,2},{4,5},{5,4},{6,7},{7,6},{8,9},{9,8},{10,11... | collective-permute-start | bytes 1572872 | tf_op jit(solution)/shard_map/ppermute | solution.py:136
  168.6 25.6 %collective-permute-start.9 = (bf16[2048,128]{1,0:T(8,128)(2,1)}, bf16[2048,128]{1,0:T(8,128)(2,1)}, u32[]{:S(2)}, u32[]{:S(2)}) collective-permute-start(bf16[2048,128]{1,0:T(8,128)(2,1)} %collective-permute-done.7.refs_2_), channel_id=1, source_target_pairs={{0,1},{1,0},{2,3},{3,2},{4,5},{5,4},{6,7},{7,6},{8,9},{9,8},{10,11... | collective-permute-start | bytes 1572872 | tf_op jit(solution)/shard_map/ppermute | solution.py:136
  171.5 17.5 %copy-start.33 = (bf16[128,2048]{1,0:T(8,128)(2,1)}, bf16[128,2048]{1,0:T(8,128)(2,1)S(1)}, u32[]{:S(2)}) copy-start(bf16[128,2048]{1,0:T(8,128)(2,1)S(1)} %collective-permute-done.14.refs_11_) | copy-start | bytes 1572868
  171.6 22.7 %collective-permute-start.32 = (bf16[40,2048]{1,0:T(8,128)(2,1)}, bf16[40,2048]{1,0:T(8,128)(2,1)S(1)}, u32[]{:S(2)}, u32[]{:S(2)}) collective-permute-start(bf16[40,2048]{1,0:T(8,128)(2,1)} %get-tuple-element.14), channel_id=1, source_target_pairs={{0,28},{4,0},{8,4},{12,8},{16,12},{20,16},{24,20},{28,24},{1,29},{... | collective-permute-start | bytes 491528 | tf_op jit(solution)/shard_map/ppermute | solution.py:22
  189.0 8.5 %collective-permute-start.33 = (bf16[40,2048]{1,0:T(8,128)(2,1)}, bf16[40,2048]{1,0:T(8,128)(2,1)}, u32[]{:S(2)}, u32[]{:S(2)}) collective-permute-start(bf16[40,2048]{1,0:T(8,128)(2,1)} %get-tuple-element.13), channel_id=1, source_target_pairs={{0,24},{4,28},{8,0},{12,4},{16,8},{20,12},{24,16},{28,20},{1,25},{... | collective-permute-start | bytes 491528 | tf_op jit(solution)/shard_map/ppermute | solution.py:22
  190.6 15.6 %collective-permute-start.34 = (bf16[40,2048]{1,0:T(8,128)(2,1)}, bf16[40,2048]{1,0:T(8,128)(2,1)S(1)}, u32[]{:S(2)}, u32[]{:S(2)}) collective-permute-start(bf16[40,2048]{1,0:T(8,128)(2,1)} %get-tuple-element.12), channel_id=1, source_target_pairs={{0,20},{4,24},{8,28},{12,0},{16,4},{20,8},{24,12},{28,16},{1,21},{... | collective-permute-start | bytes 491528 | tf_op jit(solution)/shard_map/ppermute | solution.py:22
  190.6 23.4 %collective-permute-start.35 = (bf16[40,2048]{1,0:T(8,128)(2,1)}, bf16[40,2048]{1,0:T(8,128)(2,1)S(1)}, u32[]{:S(2)}, u32[]{:S(2)}) collective-permute-start(bf16[40,2048]{1,0:T(8,128)(2,1)} %get-tuple-element.11), channel_id=1, source_target_pairs={{0,16},{4,20},{8,24},{12,28},{16,0},{20,4},{24,8},{28,12},{1,17},{... | collective-permute-start | bytes 491528 | tf_op jit(solution)/shard_map/ppermute | solution.py:22
  194.2 25.7 %collective-permute-start.36 = (bf16[40,2048]{1,0:T(8,128)(2,1)}, bf16[40,2048]{1,0:T(8,128)(2,1)S(1)}, u32[]{:S(2)}, u32[]{:S(2)}) collective-permute-start(bf16[40,2048]{1,0:T(8,128)(2,1)} %get-tuple-element.10), channel_id=1, source_target_pairs={{0,12},{4,16},{8,20},{12,24},{16,28},{20,0},{24,4},{28,8},{1,13},{... | collective-permute-start | bytes 491528 | tf_op jit(solution)/shard_map/ppermute | solution.py:22
  194.2 12.0 %copy-start.24 = (bf16[40,2048]{1,0:T(8,128)(2,1)}, bf16[40,2048]{1,0:T(8,128)(2,1)S(1)}, u32[]{:S(2)}) copy-start(bf16[40,2048]{1,0:T(8,128)(2,1)S(1)} %collective-permute-done.32.rest_1_) | copy-start | bytes 491524
  194.2 25.7 %collective-permute-start.37 = (bf16[40,2048]{1,0:T(8,128)(2,1)}, bf16[40,2048]{1,0:T(8,128)(2,1)S(1)}, u32[]{:S(2)}, u32[]{:S(2)}) collective-permute-start(bf16[40,2048]{1,0:T(8,128)(2,1)} %get-tuple-element.9), channel_id=1, source_target_pairs={{0,8},{4,12},{8,16},{12,20},{16,24},{20,28},{24,0},{28,4},{1,9},{5... | collective-permute-start | bytes 491528 | tf_op jit(solution)/shard_map/ppermute | solution.py:22
  197.5 22.4 %collective-permute-start.38 = (bf16[40,2048]{1,0:T(8,128)(2,1)S(1)}, bf16[40,2048]{1,0:T(8,128)(2,1)S(1)}, u32[]{:S(2)}, u32[]{:S(2)}) collective-permute-start(bf16[40,2048]{1,0:T(8,128)(2,1)S(1)} %get-tuple-element.8), channel_id=1, source_target_pairs={{0,4},{4,8},{8,12},{12,16},{16,20},{20,24},{24,28},{28,0},{1,5},{5... | collective-permute-start | bytes 491528 | tf_op jit(solution)/shard_map/ppermute | solution.py:22
  206.2 13.8 %copy-start.25 = (bf16[40,2048]{1,0:T(8,128)(2,1)}, bf16[40,2048]{1,0:T(8,128)(2,1)S(1)}, u32[]{:S(2)}) copy-start(bf16[40,2048]{1,0:T(8,128)(2,1)S(1)} %collective-permute-done.34.rest_3_) | copy-start | bytes 491524
  214.0 5.9 %copy-start.26 = (bf16[40,2048]{1,0:T(8,128)(2,1)}, bf16[40,2048]{1,0:T(8,128)(2,1)S(1)}, u32[]{:S(2)}) copy-start(bf16[40,2048]{1,0:T(8,128)(2,1)S(1)} %collective-permute-done.35.rest_4_) | copy-start | bytes 491524
  (15 other events, 18.4 us)
Sparse Core Ops, SparseCore 0:
  138.8 34.9 reduce-scatter.1
